TPU v7x, 32 devices: a whole 2x2x4 slice. The times are simulated.
32 devices in a mesh: sp: 4 (over y, x), tp: 8 (over z, core).
Axes of the slice: x: 2, y: 2, z: 4, core: 2. Of those that a mesh axis runs over, the one named last changes fastest.
Arguments:
- upstream: bfloat16 [1024, 4096], P('sp', 'tp'), may hold values from -6 to 6
- stream: bfloat16 [1024, 4096], P('sp', 'tp'), may hold values from -400 to 400
- norm_gain: float32 [4096], P('tp'), may hold values from 0.1 to 1.9
- routes: int32 [1024, 2], P('sp'), may hold values from 0 to 3, all different within a row; in each aligned block of 256 rows (0 to 255, 256 to 511, ...) at most 192 rows name the same one
- route_weights: float32 [1024, 2], P('sp'), may hold values from 0.1 to 1
- w_gate: bfloat16 [4, 4096, 2048], P('sp', None, 'tp'), may hold values from -0.09375 to 0.09375
- w_up: bfloat16 [4, 4096, 2048], P('sp', None, 'tp'), may hold values from -0.09375 to 0.09375
- w_down: bfloat16 [4, 2048, 4096], P('sp', 'tp'), may hold values from -0.125 to 0.125
- value_in: bfloat16 [1024, 2048], P('sp', 'tp'), may hold values from -6 to 6
- gate_in: bfloat16 [1024, 2048], P('sp', 'tp'), may hold values from -6 to 6
- conv_pre: bfloat16 [1024, 2048], P('sp', 'tp'), may hold values from -200 to 200
- ln_gain: float32 [2048], P('tp'), may hold values from 0.1 to 1.9
- conv_taps: float32 [31, 2048], P(None, 'tp'), may hold values from -1 to 1
- w_out: bfloat16 [2048, 4096], P('tp'), may hold values from -0.125 to 0.125
Outputs:
- grad_gate: float32 [4, 4096, 2048], P('sp', None, 'tp')
- grad_up: float32 [4, 4096, 2048], P('sp', None, 'tp')
- grad_down: float32 [4, 2048, 4096], P('sp', 'tp')
- grad_out: float32 [2048, 4096], P('tp', 'sp')
- value_grad: bfloat16 [1024, 2048], P('sp', 'tp')
- gate_grad: bfloat16 [1024, 2048], P('sp', 'tp')
Inputs may be any that keep to these rules, and one draw needn't show every extreme that they name: `routes`: each token names two different experts. Among the tokens of one index of sp no expert is named more than 192 times, and in every draw some expert exactly 192 times.
All inputs are finite; a program needn't handle non-finite values.
Results may differ from a plain program's by a relative error of at most 0.0071.
Values may be sent and summed in bfloat16 or wider, within the bound.
A program may use at most 128 MiB of HBM per device.

v0:
```python
import functools

import jax
import jax.numpy as jnp
from jax import lax
from jax.experimental import pallas as pl
from jax.experimental.pallas import tpu as pltpu
from jax.sharding import PartitionSpec as P


EPSILON = 1e-06
VMEM_LIMIT = 60 * 2**20


def shifted(block, axis, distance):
    devices = range(lax.axis_size(axis))
    route = [(i - distance, i) for i in devices if i - distance in devices]
    return lax.ppermute(block, axis, route)


def group_sum_kernel(axis, group, own_ref, out_ref, landed, send_sems, recv_sems):
    me = lax.axis_index(axis)
    barrier = pltpu.get_barrier_semaphore()
    for step in range(1, group):
        pl.semaphore_signal(
            barrier,
            inc=1,
            device_id={axis: lax.rem(me + step, group)},
            device_id_type=pl.DeviceIdType.MESH,
        )
    pl.semaphore_wait(barrier, group - 1)
    copies = []
    for step in range(1, group):
        copy = pltpu.make_async_remote_copy(
            src_ref=own_ref,
            dst_ref=landed.at[step - 1],
            send_sem=send_sems.at[step - 1],
            recv_sem=recv_sems.at[step - 1],
            device_id={axis: lax.rem(me + step, group)},
            device_id_type=pl.DeviceIdType.MESH,
        )
        copy.start()
        copies.append(copy)
    for copy in copies:
        copy.wait()
    total = own_ref[...]
    for step in range(1, group):
        total = total + landed[step - 1]
    out_ref[...] = total


def group_sum(vectors, axis, collective_id):
    block = jnp.stack(vectors, axis=0)
    group = lax.axis_size(axis)
    summed = pl.pallas_call(
        functools.partial(group_sum_kernel, axis, group),
        out_shape=jax.ShapeDtypeStruct(block.shape, block.dtype),
        in_specs=[pl.BlockSpec(memory_space=pltpu.VMEM)],
        out_specs=pl.BlockSpec(memory_space=pltpu.VMEM),
        scratch_shapes=[
            pltpu.VMEM((group - 1,) + block.shape, block.dtype),
            pltpu.SemaphoreType.DMA((group - 1,)),
            pltpu.SemaphoreType.DMA((group - 1,)),
        ],
        compiler_params=pltpu.CompilerParams(
            collective_id=collective_id, has_side_effects=True
        ),
        cost_estimate=pl.CostEstimate(
            flops=group * block.size, bytes_accessed=400 * block.size * 4, transcendentals=0
        ),
        name="group_sum",
    )(block)
    return tuple(summed[row] for row in range(len(vectors)))


def silu_slope(values):
    logistic = jax.nn.sigmoid(values)
    return logistic * (1.0 + values * (1.0 - logistic))


def per_device(
    upstream,
    stream,
    norm_gain,
    routes,
    route_weights,
    w_gate,
    w_up,
    w_down,
    value_in,
    gate_in,
    conv_pre,
    ln_gain,
    conv_taps,
    w_out,
):
    tok_rows, width_part = stream.shape
    token_groups = lax.axis_size("sp")
    width_groups = lax.axis_size("tp")
    model_width = width_part * width_groups
    channels = conv_pre.shape[1] * width_groups
    tap_count = conv_taps.shape[0]
    capacity = 3 * tok_rows // token_groups
    experts = w_gate.shape[0] * token_groups
    slot_count = experts * capacity
    expert_rows = token_groups * capacity
    flat_experts = routes.reshape(-1)
    one_hot = (flat_experts[:, None] == jnp.arange(experts, dtype=jnp.int32)[None, :]).astype(
        jnp.int32
    )
    slot_rank = jnp.sum((jnp.cumsum(one_hot, axis=0) - one_hot) * one_hot, axis=1)
    slot_index = (flat_experts * capacity + slot_rank).reshape(tok_rows, 2)
    slot_ids = jnp.arange(slot_count, dtype=jnp.int32)[:, None]
    first_hit = slot_ids == slot_index[None, :, 0]
    second_hit = slot_ids == slot_index[None, :, 1]
    any_hit = jnp.logical_or(first_hit, second_hit)
    picker = any_hit.astype(jnp.bfloat16)
    slot_weight = jnp.sum(
        jnp.where(first_hit, route_weights[None, :, 0], 0.0)
        + jnp.where(second_hit, route_weights[None, :, 1], 0.0),
        axis=1,
    )
    token_iota = jnp.arange(tok_rows, dtype=jnp.int32)[None, :]
    slot_token = jnp.where(
        jnp.any(any_hit, axis=1), jnp.sum(jnp.where(any_hit, token_iota, 0), axis=1), tok_rows
    )
    columns = stream.shape[1]
    spare = jnp.zeros((1, columns), jnp.bfloat16)
    upstream_pad = jnp.concatenate([upstream, spare], axis=0)
    cotangent = (upstream_pad[slot_token].astype(jnp.float32) * slot_weight[:, None]).astype(
        jnp.bfloat16
    )
    sent_cotangent = cotangent.reshape(experts, capacity, columns)
    part_cotangent = lax.all_to_all(
        sent_cotangent, "sp", split_axis=0, concat_axis=0, tiled=True
    ).reshape(expert_rows, width_part)
    part_cotangent, stream_late, conv_late = lax.optimization_barrier(
        (part_cotangent, stream, conv_pre)
    )
    cotangent = lax.all_gather(part_cotangent, "tp", axis=1, tiled=True)
    residual = stream_late.astype(jnp.float32)
    conv_vals = conv_late.astype(jnp.float32)
    row_squares, conv_total, conv_squares = group_sum(
        (
            jnp.sum(residual * residual, axis=1),
            jnp.sum(conv_vals, axis=1),
            jnp.sum(conv_vals * conv_vals, axis=1),
        ),
        "tp",
        0,
    )
    inverse = lax.rsqrt(row_squares / model_width + EPSILON)[:, None]
    normed = (norm_gain[None, :] * residual * inverse).astype(jnp.bfloat16)
    normed_pad = jnp.concatenate([normed, spare], axis=0)
    inputs = normed_pad[slot_token]
    sent_inputs = inputs.reshape(experts, capacity, columns)
    part_inputs = lax.all_to_all(sent_inputs, "sp", split_axis=0, concat_axis=0, tiled=True)
    inputs = lax.all_gather(
        part_inputs.reshape(expert_rows, width_part), "tp", axis=1, tiled=True
    )
    gate_mat = w_gate[0]
    upper_mat = w_up[0]
    down_mat = w_down[0]
    gate_pre = jnp.dot(inputs, gate_mat, preferred_element_type=jnp.float32)
    upper_pre = jnp.dot(inputs, upper_mat, preferred_element_type=jnp.float32)
    active = (jax.nn.silu(gate_pre) * upper_pre).astype(jnp.bfloat16)
    active_back = lax.dot_general(
        cotangent, down_mat, (((1,), (1,)), ((), ())), preferred_element_type=jnp.float32
    )
    gate_back = (active_back * upper_pre * silu_slope(gate_pre)).astype(jnp.bfloat16)
    upper_back = (active_back * jax.nn.silu(gate_pre)).astype(jnp.bfloat16)
    grad_gate = lax.dot_general(
        inputs, gate_back, (((0,), (0,)), ((), ())), preferred_element_type=jnp.float32
    )
    grad_up = lax.dot_general(
        inputs, upper_back, (((0,), (0,)), ((), ())), preferred_element_type=jnp.float32
    )
    grad_down = lax.dot_general(
        active, cotangent, (((0,), (0,)), ((), ())), preferred_element_type=jnp.float32
    )
    input_part = lax.dot_general(
        gate_back, gate_mat, (((1,), (1,)), ((), ())), preferred_element_type=jnp.float32
    ) + lax.dot_general(
        upper_back, upper_mat, (((1,), (1,)), ((), ())), preferred_element_type=jnp.float32
    )
    input_back = lax.psum_scatter(
        input_part.astype(jnp.bfloat16), "tp", scatter_dimension=1, tiled=True
    )
    input_back, grad_gate, grad_up, grad_down = lax.optimization_barrier(
        (input_back, grad_gate, grad_up, grad_down)
    )
    returned = lax.all_to_all(
        input_back.reshape(token_groups, capacity, width_part),
        "sp",
        split_axis=0,
        concat_axis=0,
        tiled=True,
    )
    returned = returned.reshape(slot_count, width_part)
    token_back = lax.dot_general(
        picker, returned, (((0,), (0,)), ((), ())), preferred_element_type=jnp.float32
    )
    gained = norm_gain[None, :] * token_back
    (inner_sum,) = group_sum((jnp.sum(gained * residual, axis=1),), "tp", 1)
    norm_back = inverse * gained - residual * inverse**3 * (inner_sum / model_width)[:, None]
    stream_grad = (upstream.astype(jnp.float32) + norm_back).astype(jnp.bfloat16)
    full_grad = lax.all_gather(stream_grad, "tp", axis=1, tiled=True)
    mean_val = (conv_total / channels)[:, None]
    variance = (conv_squares / channels)[:, None] - mean_val * mean_val
    inv_std = lax.rsqrt(variance + EPSILON)
    centred = (conv_vals - mean_val) * inv_std
    scaled = centred * ln_gain[None, :]
    mixed_out = jax.nn.silu(scaled).astype(jnp.bfloat16)
    grad_rows = lax.dot_general(
        full_grad, mixed_out, (((0,), (0,)), ((), ())), preferred_element_type=jnp.float32
    ).astype(jnp.bfloat16)
    grad_out = (
        lax.psum_scatter(grad_rows, "sp", scatter_dimension=0, tiled=True).astype(jnp.float32).T
    )
    mixed_back = lax.dot_general(
        full_grad, w_out, (((1,), (1,)), ((), ())), preferred_element_type=jnp.float32
    )
    norm_in = mixed_back * silu_slope(scaled) * ln_gain[None, :]
    norm_total, norm_cross = group_sum(
        (jnp.sum(norm_in, axis=1), jnp.sum(norm_in * centred, axis=1)), "tp", 2
    )
    conv_back = inv_std * (
        norm_in - (norm_total / channels)[:, None] - centred * (norm_cross / channels)[:, None]
    )
    next_rim = shifted(conv_back[: tap_count - 1], "sp", -1)
    padded = jnp.concatenate([conv_back, next_rim], axis=0)
    glu_back = jnp.zeros(conv_back.shape, jnp.float32)
    for tap_index in range(tap_count):
        offset = tap_count - 1 - tap_index
        glu_back = glu_back + conv_taps[tap_index][None, :] * padded[offset : offset + tok_rows]
    gate_sigma = jax.nn.sigmoid(gate_in.astype(jnp.float32))
    value_grad = (glu_back * gate_sigma).astype(jnp.bfloat16)
    gate_grad = (glu_back * value_in.astype(jnp.float32) * gate_sigma * (1.0 - gate_sigma)).astype(
        jnp.bfloat16
    )
    return (grad_gate[None], grad_up[None], grad_down[None], grad_out, value_grad, gate_grad)


MESH_ID = pl.DeviceIdType.MESH


def remote(src, dst, send_sem, recv_sem, sp_index, tp_index):
    return pltpu.make_async_remote_copy(
        src_ref=src,
        dst_ref=dst,
        send_sem=send_sem,
        recv_sem=recv_sem,
        device_id={"sp": sp_index, "tp": tp_index},
        device_id_type=MESH_ID,
    )


def greet(devices):
    barrier = pltpu.get_barrier_semaphore()
    for sp_index, tp_index in devices:
        pl.semaphore_signal(
            barrier,
            inc=1,
            device_id={"sp": sp_index, "tp": tp_index},
            device_id_type=MESH_ID,
        )
    pl.semaphore_wait(barrier, len(devices))


def places():
    sp = lax.axis_index("sp")
    tp = lax.axis_index("tp")
    chip, core = tp // 2, tp % 2
    side = 1 - 2 * (sp % 2)
    lift = 2 - 4 * (sp // 2)
    across, along = sp + side, sp + lift
    corner = 3 - sp
    hops = (
        chip,
        chip + 1 - 2 * (chip % 2),
        chip + 2 - 4 * (chip // 2),
        3 - chip,
    )
    return sp, tp, chip, core, across, along, corner, hops


def to_column(row):
    count = row.shape[1]
    down = lax.broadcasted_iota(jnp.int32, (count, count), 0)
    over = lax.broadcasted_iota(jnp.int32, (count, count), 1)
    return jnp.sum(jnp.where(down == over, row, 0.0), axis=1, keepdims=True)


def to_row(column):
    count = column.shape[0]
    down = lax.broadcasted_iota(jnp.int32, (count, count), 0)
    over = lax.broadcasted_iota(jnp.int32, (count, count), 1)
    return jnp.sum(jnp.where(down == over, column, 0.0), axis=0, keepdims=True)


def dot_nt(left, right):
    return lax.dot_general(
        left, right, (((1,), (1,)), ((), ())), preferred_element_type=jnp.float32
    )


def dot_tn(left, right):
    return lax.dot_general(
        left, right, (((0,), (0,)), ((), ())), preferred_element_type=jnp.float32
    )


def expert_kernel(
    width,
    gs_ref,
    up_ref,
    stat_ref,
    wrow_ref,
    wg_hbm,
    wu_hbm,
    wd_hbm,
    rows_s,
    rows_u,
    hidden,
    active,
    keep,
    send_x,
    send_y,
    stat_out,
    wgu,
    wd,
    mate_w,
    mate_h,
    acc,
    back,
    stat_in,
    inv_out,
    inv_in,
    w_in,
    z_send,
    piece_recv,
    xy_send,
    relay_send,
    mate_send,
    mate_recv,
    stat_send,
    stat_recv,
    inv_send,
    inv_recv,
    w_send,
    w_recv,
    mw_sems,
    mh_send,
    mh_recv,
    local_sems,
):
    sp, tp, chip, core, across, along, corner, hops = places()
    mate = tp + 1 - 2 * core
    tokens, columns = gs_ref.shape
    part = wd_hbm.shape[0]
    tp_count = 8
    peers = [lax.rem(tp + step, tp_count) for step in range(1, tp_count)]
    others = (across, along, corner)
    owns = (gs_ref, up_ref)
    rows = (rows_s, rows_u)

    loads = [
        pltpu.make_async_copy(wg_hbm, wgu.at[:, :, :, pl.ds(0, part)], local_sems.at[0]),
        pltpu.make_async_copy(wu_hbm, wgu.at[:, :, :, pl.ds(part, part)], local_sems.at[1]),
        pltpu.make_async_copy(wd_hbm, wd, local_sems.at[2]),
        pltpu.make_async_copy(gs_ref, rows_s.at[sp, core, chip], local_sems.at[3]),
        pltpu.make_async_copy(up_ref, rows_u.at[sp, core, chip], local_sems.at[4]),
    ]
    for load in loads:
        load.start()
    greet([(sp, peer) for peer in peers] + [(other, tp) for other in others])

    pending = []

    def go(copy):
        copy.start()
        pending.append(copy)

    for i, peer in enumerate(peers):
        go(remote(stat_ref, stat_in.at[tp], stat_send.at[i], stat_recv.at[tp], sp, peer))
    for i, other in enumerate(others):
        go(remote(wrow_ref.at[other], w_in.at[sp], w_send.at[i], w_recv.at[sp], other, tp))

    def send_piece(kind, step, source):
        place = hops[step]
        for way, target in enumerate((across, along)):
            go(
                remote(
                    source,
                    rows[kind].at[sp, core, place],
                    xy_send.at[kind, step, way],
                    piece_recv.at[kind, sp, place],
                    target,
                    tp,
                )
            )

    for kind in (0, 1):
        for step in (1, 2, 3):
            go(
                remote(
                    owns[kind],
                    rows[kind].at[sp, core, chip],
                    z_send.at[kind, step - 1],
                    piece_recv.at[kind, sp, chip],
                    sp,
                    2 * hops[step] + core,
                )
            )
        send_piece(kind, 0, owns[kind])

    def await_piece(kind, origin, step):
        slot = rows[kind].at[origin, core, hops[step]]
        remote(
            slot,
            slot,
            mate_send.at[kind, origin],
            piece_recv.at[kind, origin, hops[step]],
            sp,
            mate,
        ).wait_recv()

    def relay(kind, step):
        origin, target = (across, along) if step % 2 == 0 else (along, across)
        await_piece(kind, origin, step)
        slot = rows[kind].at[origin, core, hops[step]]
        go(
            remote(
                slot,
                slot,
                relay_send.at[kind, step],
                piece_recv.at[kind, origin, hops[step]],
                target,
                tp,
            )
        )

    def share(kind, origin):
        slot = rows[kind].at[origin, core]
        go(
            remote(
                slot, slot, mate_send.at[kind, origin], mate_recv.at[kind, origin], sp, mate
            )
        )

    def await_share(kind, origin):
        slot = rows[kind].at[origin, 1 - core]
        remote(
            slot, slot, mate_send.at[kind, origin], mate_recv.at[kind, origin], sp, mate
        ).wait_recv()

    for load in loads:
        load.wait()
    go(
        remote(
            wgu.at[:, 1 - core], mate_w, mw_sems.at[0], mw_sems.at[1], sp, mate
        )
    )
    acc[...] = jnp.zeros(acc.shape, jnp.float32)
    back[...] = jnp.zeros(back.shape, jnp.float32)
    w_in[sp] = wrow_ref[sp]

    total = stat_ref[...]
    for peer in peers:
        remote(
            stat_in.at[peer], stat_in.at[peer], stat_send.at[0], stat_recv.at[peer], sp, peer
        ).wait_recv()
        total = total + stat_in[peer]
    stat_out[...] = total
    inverse_row = lax.rsqrt(total[0:1] / width + EPSILON)
    inv_out[...] = jnp.broadcast_to(inverse_row, inv_out.shape)
    inv_in[sp] = jnp.broadcast_to(inverse_row, inv_out.shape)
    for i, other in enumerate(others):
        go(remote(inv_out, inv_in.at[sp], inv_send.at[i], inv_recv.at[sp], other, tp))

    def forward(origin):
        def body(index, carry):
            half, place = index // 4, lax.rem(index, 4)
            acc[origin] += jnp.dot(
                rows_s[origin, half, place],
                wgu[place, half],
                preferred_element_type=jnp.float32,
            )
            return carry

        lax.fori_loop(0, tp_count, body, 0)

    def backward(origin, half):
        def body(place, carry):
            start = pl.multiple_of((2 * place + half) * columns, columns)
            back[origin] += dot_nt(rows_u[origin, half, place], wd[:, pl.ds(start, columns)])
            return carry

        lax.fori_loop(0, 4, body, 0)

    chunk = 64

    def activate(origin):
        inverse = to_column(inv_in[origin, 0:1])
        weight = to_column(w_in[origin, 0:1])
        for begin in range(0, tokens, chunk):
            end = begin + chunk
            pre = acc[origin, begin:end] * inverse[begin:end]
            gate, upper = pre[:, :part], pre[:, part:]
            cot = back[origin, begin:end] * weight[begin:end]
            logistic = 1.0 / (1.0 + jnp.exp(-gate))
            silu = gate * logistic
            slope = logistic * (1.0 + gate * (1.0 - logistic))
            active[origin, begin:end] = (silu * upper * weight[begin:end]).astype(jnp.bfloat16)
            back_inv = cot * inverse[begin:end]
            hidden[origin, begin:end, :part] = (back_inv * upper * slope).astype(jnp.bfloat16)
            hidden[origin, begin:end, part:] = (back_inv * silu).astype(jnp.bfloat16)
        go(
            remote(
                hidden.at[origin],
                mate_h.at[origin],
                mh_send.at[origin],
                mh_recv.at[origin],
                sp,
                mate,
            )
        )

    def spread(origin, low, high):
        remote(
            mate_h.at[origin],
            mate_h.at[origin],
            mh_send.at[origin],
            mh_recv.at[origin],
            sp,
            mate,
        ).wait_recv()

        for target, first in ((low, 0), (high, 2)):

            def body(i, carry, target=target, first=first):
                place = first + i
                part_sum = dot_nt(hidden[origin], wgu[place, core]) + dot_nt(
                    mate_h[origin], mate_w[place]
                )
                target[i] = part_sum.astype(jnp.bfloat16)
                return carry

            lax.fori_loop(0, 2, body, 0)

    def arrive(kind, step):
        await_piece(kind, sp, step)
        send_piece(kind, step, rows[kind].at[sp, core, hops[step]])

    arrive(0, 1)
    relay(0, 0)
    arrive(0, 2)
    relay(1, 0)
    arrive(0, 3)
    relay(0, 1)
    share(0, sp)
    arrive(1, 1)
    relay(0, 2)
    await_share(0, sp)
    forward(sp)
    arrive(1, 2)
    relay(0, 3)
    for step in (1, 3):
        await_piece(0, across, step)
    share(0, across)
    for step in (0, 2):
        await_piece(0, along, step)
    share(0, along)
    arrive(1, 3)
    relay(1, 1)
    share(1, sp)
    await_share(0, across)
    forward(across)
    await_share(0, along)
    forward(along)
    relay(1, 2)
    for step in (0, 1, 2, 3):
        await_piece(0, corner, step)
    share(0, corner)
    await_share(1, sp)
    backward(sp, 0)
    backward(sp, 1)
    await_share(0, corner)
    forward(corner)
    relay(1, 3)
    for other in others:
        for sems, landing in ((inv_recv, inv_in), (w_recv, w_in)):
            remote(
                landing.at[other], landing.at[other], inv_send.at[0], sems.at[other], sp, mate
            ).wait_recv()
    activate(sp)
    for step in (1, 3):
        await_piece(1, across, step)
    share(1, across)
    for step in (0, 2):
        await_piece(1, along, step)
    share(1, along)
    remote(mate_w, mate_w, mw_sems.at[0], mw_sems.at[1], sp, mate).wait_recv()
    await_share(1, across)
    backward(across, 0)
    backward(across, 1)
    activate(across)
    await_share(1, along)
    backward(along, 0)
    backward(along, 1)
    activate(along)
    row_of = sp // 2
    col_of = lax.rem(sp, 2)
    spread(sp, keep.at[0, row_of], keep.at[1, col_of])
    spread(across, send_x.at[row_of], keep.at[1, 1 - col_of])
    spread(along, keep.at[0, 1 - row_of], send_y.at[col_of])
    for step in (0, 1, 2, 3):
        await_piece(1, corner, step)
    share(1, corner)
    backward(corner, core)
    await_share(1, corner)
    backward(corner, 1 - core)
    activate(corner)
    spread(corner, send_x.at[1 - row_of], send_y.at[1 - col_of])
    for copy in pending:
        copy.wait_send()


def grads_kernel(rows_s, rows_u, hidden, active, gate_out, up_out, down_out, tall, wide, sems):
    columns = rows_s.shape[4]
    part = active.shape[2]
    pieces = 8

    def copies(piece, slot):
        span = pl.ds(pl.multiple_of(piece * columns, columns), columns)
        return (
            pltpu.make_async_copy(
                tall.at[slot, :, pl.ds(0, part)], gate_out.at[span], sems.at[slot, 0]
            ),
            pltpu.make_async_copy(
                tall.at[slot, :, pl.ds(part, part)], up_out.at[span], sems.at[slot, 1]
            ),
            pltpu.make_async_copy(wide.at[slot], down_out.at[:, span], sems.at[slot, 2]),
        )

    def body(piece, carry):
        slot = lax.rem(piece, 2)
        half, place = lax.rem(piece, 2), piece // 2

        @pl.when(piece >= 2)
        def _():
            for copy in copies(piece - 2, slot):
                copy.wait()

        for origin in range(4):
            tall_term = dot_tn(rows_s[origin, half, place], hidden[origin])
            wide_term = dot_tn(active[origin], rows_u[origin, half, place])
            if origin == 0:
                tall[slot] = tall_term
                wide[slot] = wide_term
            else:
                tall[slot] += tall_term
                wide[slot] += wide_term
        for copy in copies(piece, slot):
            copy.start()
        return carry

    lax.fori_loop(0, pieces, body, 0)
    for piece in (pieces - 2, pieces - 1):
        for copy in copies(piece, piece % 2):
            copy.wait()


def return_kernel(
    width,
    channels,
    keep,
    got_x,
    got_y,
    up_ref,
    stream_ref,
    gain_ref,
    inv_ref,
    mixed_ref,
    slope_ref,
    centred_ref,
    invstd_ref,
    w_hbm,
    conv_out,
    grads,
    mixed,
    w_out,
    turn_out,
    turn_in,
    z_out,
    z_in,
    own_sum,
    note_out,
    note_in,
    tail_out,
    tail_in,
    full,
    rim_in,
    mix_send,
    mix_recv,
    turn_send,
    turn_recv,
    z_send,
    z_recv,
    note_send,
    note_recv,
    tail_send,
    tail_recv,
    full_send,
    full_recv,
    mate_send,
    mate_recv,
    grad_send,
    grad_recv,
    gmate_send,
    gmate_recv,
    rim_sems,
    local_sems,
):
    sp, tp, chip, core, across, along, corner, hops = places()
    mate = tp + 1 - 2 * core
    tp_count = 8
    tokens, columns = up_ref.shape
    row_of = sp // 2
    col_of = lax.rem(sp, 2)
    peers = [lax.rem(tp + step, tp_count) for step in range(1, tp_count)]
    others = (across, along, corner)
    load = pltpu.make_async_copy(w_hbm, w_out, local_sems.at[0])
    load.start()
    own_mixed = pltpu.make_async_copy(mixed_ref, mixed.at[sp], local_sems.at[1])
    own_mixed.start()
    greet([(sp, peer) for peer in peers] + [(other, tp) for other in others])
    pending = []

    def go(copy):
        copy.start()
        pending.append(copy)

    turns = ((0, 1 - row_of, row_of, got_x, along), (1, 1 - col_of, col_of, got_y, across))
    for i in range(2):
        for group, far, near, got, target in turns:
            turn_out[group, i] = (
                keep[group, far, i].astype(jnp.float32) + got[far, i].astype(jnp.float32)
            ).astype(jnp.bfloat16)
            go(
                remote(
                    turn_out.at[group, i],
                    turn_in.at[group, i],
                    turn_send.at[group, i],
                    turn_recv.at[group, i],
                    target,
                    tp,
                )
            )
    for i, other in enumerate(others):
        go(remote(mixed_ref, mixed.at[sp], mix_send.at[i], mix_recv.at[sp], other, tp))
    for i in range(2):
        for group, far, near, got, target in turns:
            place = 2 * group + i
            remote(
                turn_in.at[group, i],
                turn_in.at[group, i],
                turn_send.at[group, i],
                turn_recv.at[group, i],
                target,
                tp,
            ).wait_recv()
            summed = (
                keep[group, near, i].astype(jnp.float32)
                + got[near, i].astype(jnp.float32)
                + turn_in[group, i].astype(jnp.float32)
            )

            @pl.when(chip == place)
            def _(summed=summed):
                own_sum[...] = summed

            @pl.when(chip != place)
            def _(summed=summed, place=place):
                z_out[place] = summed.astype(jnp.bfloat16)
                remote(
                    z_out.at[place],
                    z_in.at[chip],
                    z_send.at[place],
                    z_recv.at[chip],
                    sp,
                    2 * place + core,
                ).start()

    for step in (1, 2, 3):
        place = hops[step]
        remote(
            z_out.at[place], z_in.at[place], z_send.at[place], z_recv.at[place], sp, mate
        ).wait()

    gain = gain_ref[...]
    chunk = 64
    for begin in range(0, tokens, chunk):
        end = begin + chunk
        own_sum[begin:end] = gain * (
            own_sum[begin:end]
            + z_in[hops[1], begin:end].astype(jnp.float32)
            + z_in[hops[2], begin:end].astype(jnp.float32)
            + z_in[hops[3], begin:end].astype(jnp.float32)
        )
    inner = jnp.sum(own_sum[...] * stream_ref[...].astype(jnp.float32), axis=1, keepdims=True)
    inner_row = to_row(inner)
    note_out[...] = jnp.broadcast_to(inner_row, note_out.shape)
    for i, peer in enumerate(peers):
        go(remote(note_out, note_in.at[tp], note_send.at[i], note_recv.at[tp], sp, peer))
    for peer in peers:
        remote(
            note_in.at[peer], note_in.at[peer], note_send.at[0], note_recv.at[peer], sp, peer
        ).wait_recv()
        inner_row = inner_row + note_in[peer, 0:1]
    inverse = inv_ref[...]
    factor = inverse * inverse * to_column(inner_row) / width
    for begin in range(0, tokens, chunk):
        end = begin + chunk
        full[core, chip, begin:end] = (
            up_ref[begin:end].astype(jnp.float32)
            + own_sum[begin:end]
            - stream_ref[begin:end].astype(jnp.float32) * factor[begin:end]
        ).astype(jnp.bfloat16)
    slot = full.at[core, chip]
    for step in (1, 2, 3):
        go(
            remote(
                slot,
                slot,
                full_send.at[step - 1],
                full_recv.at[chip],
                sp,
                2 * hops[step] + core,
            )
        )

    def fan(step):
        place = hops[step]
        slot = full.at[core, place]
        if step > 0:
            remote(slot, slot, full_send.at[0], full_recv.at[place], sp, mate).wait_recv()
        remote(slot, slot, mate_send.at[place], mate_recv.at[place], sp, mate).start()

        @pl.when(place != sp)
        def _():
            remote(
                slot, grads.at[sp, core], grad_send.at[place], grad_recv.at[sp], place, tp
            ).start()

    load.wait()

    def mixed_term(half, place):
        start = pl.multiple_of((2 * place + half) * columns, columns)
        return dot_nt(full[half, place], w_out[:, pl.ds(start, columns)])

    mixed_back = None
    for step in range(4):
        fan(step)
        term = mixed_term(core, hops[step])
        mixed_back = term if mixed_back is None else mixed_back + term
    for step in range(4):
        place = hops[step]
        slot = full.at[1 - core, place]
        remote(slot, slot, mate_send.at[place], mate_recv.at[place], sp, mate).wait_recv()
        mixed_back = mixed_back + mixed_term(1 - core, place)
    norm_in = mixed_back * slope_ref[...]
    centred = centred_ref[...]
    sums = jnp.concatenate(
        [
            to_row(jnp.sum(norm_in, axis=1, keepdims=True)),
            to_row(jnp.sum(norm_in * centred, axis=1, keepdims=True)),
            jnp.zeros((6, tokens), jnp.float32),
        ],
        axis=0,
    )
    tail_out[...] = sums
    for i, peer in enumerate(peers):
        go(remote(tail_out, tail_in.at[tp], tail_send.at[i], tail_recv.at[tp], sp, peer))
    for peer in peers:
        remote(
            tail_in.at[peer], tail_in.at[peer], tail_send.at[0], tail_recv.at[peer], sp, peer
        ).wait_recv()
        sums = sums + tail_in[peer]
    conv_out[0:tokens] = invstd_ref[...] * (
        norm_in - to_column(sums[0:1]) / channels - centred * (to_column(sums[1:2]) / channels)
    )
    rim = rim_in.shape[0]
    before = lax.rem(sp + 3, 4)
    go(
        remote(
            conv_out.at[pl.ds(0, rim)], rim_in, rim_sems.at[0], rim_sems.at[1], before, tp
        )
    )
    for half in range(2):
        grads[sp, half] = full[half, sp]
    for other in others:
        slot = grads.at[other, core]
        remote(slot, slot, grad_send.at[0], grad_recv.at[other], other, tp).wait_recv()
        go(remote(slot, slot, gmate_send.at[other], gmate_recv.at[other], sp, mate))
    own_mixed.wait()
    for other in others:
        slot = mixed.at[other]
        remote(slot, slot, mix_send.at[0], mix_recv.at[other], other, tp).wait_recv()
    for other in others:
        slot = grads.at[other, 1 - core]
        remote(slot, slot, gmate_send.at[other], gmate_recv.at[other], sp, mate).wait_recv()
    remote(rim_in, rim_in, rim_sems.at[0], rim_sems.at[1], before, tp).wait_recv()
    last = (sp < 3).astype(jnp.float32)
    conv_out[tokens : tokens + rim] = rim_in[...] * last
    for step in range(4):
        place = hops[step]
        slot = full.at[core, place]
        remote(slot, slot, mate_send.at[place], mate_recv.at[place], sp, mate).wait_send()

        @pl.when(place != sp)
        def _(slot=slot, place=place):
            remote(
                slot, grads.at[sp, core], grad_send.at[place], grad_recv.at[sp], place, tp
            ).wait_send()

    for copy in pending:
        copy.wait_send()


def finish_kernel(conv, taps, value_in, gate_in, grads, mixed, grad_out, value_out, gate_out):
    tokens, part = value_in.shape
    tap_count = taps.shape[0]
    columns = grads.shape[3]
    for half in range(2):
        total = dot_tn(mixed[0], grads[0, half])
        for origin in range(1, 4):
            total = total + dot_tn(mixed[origin], grads[origin, half])
        grad_out[:, half * columns : (half + 1) * columns] = total
    glu = jnp.zeros((tokens, part), jnp.float32)
    for residue in range(8):
        rolled = None
        for offset in range(residue, tap_count, 8):
            base = offset - residue
            tap = taps[tap_count - 1 - offset : tap_count - offset]
            term = tap * conv[base : base + tokens + 8]
            rolled = term if rolled is None else rolled + term
        glu = glu + rolled[residue : residue + tokens]
    sigma = 1.0 / (1.0 + jnp.exp(-gate_in[...].astype(jnp.float32)))
    value_out[...] = (glu * sigma).astype(jnp.bfloat16)
    gate_out[...] = (
        glu * value_in[...].astype(jnp.float32) * sigma * (1.0 - sigma)
    ).astype(jnp.bfloat16)


def fused_device(
    upstream,
    stream,
    norm_gain,
    routes,
    route_weights,
    w_gate,
    w_up,
    w_down,
    value_in,
    gate_in,
    conv_pre,
    ln_gain,
    conv_taps,
    w_out,
):
    tokens, columns = stream.shape
    tp_count = lax.axis_size("tp")
    sp_count = lax.axis_size("sp")
    chips = tp_count // 2
    width = columns * tp_count
    part = w_gate.shape[2]
    channel_part = conv_pre.shape[1]
    channels = channel_part * tp_count
    bf16, f32 = jnp.bfloat16, jnp.float32
    vmem = pl.BlockSpec(memory_space=pltpu.VMEM)
    anywhere = pl.BlockSpec(memory_space=pl.ANY)
    dma = pltpu.SemaphoreType.DMA
    shape = jax.ShapeDtypeStruct

    residual = stream.astype(f32)
    scaled_stream = (norm_gain[None, :] * residual).astype(bf16)
    conv_vals = conv_pre.astype(f32)
    stats = jnp.stack(
        [
            jnp.sum(residual * residual, axis=1),
            jnp.sum(conv_vals, axis=1),
            jnp.sum(conv_vals * conv_vals, axis=1),
        ]
        + [jnp.zeros((tokens,), f32)] * 5,
        axis=0,
    )
    expert_ids = jnp.arange(sp_count, dtype=jnp.int32)
    weights = jnp.sum(
        jnp.where(routes[None] == expert_ids[:, None, None], route_weights[None], 0.0), axis=2
    )
    weight_rows = jnp.broadcast_to(weights[:, None, :], (sp_count, 8, tokens))
    piece = (chips, 2, columns, part)
    rows_shape = (sp_count, 2, chips, tokens, columns)
    outs = pl.pallas_call(
        functools.partial(expert_kernel, width),
        out_shape=(
            shape(rows_shape, bf16),
            shape(rows_shape, bf16),
            shape((sp_count, tokens, 2 * part), bf16),
            shape((sp_count, tokens, part), bf16),
            shape((2, 2, 2, tokens, columns), bf16),
            shape((2, 2, tokens, columns), bf16),
            shape((2, 2, tokens, columns), bf16),
            shape((8, tokens), f32),
        ),
        in_specs=[vmem, vmem, vmem, vmem, anywhere, anywhere, anywhere],
        out_specs=[vmem] * 8,
        scratch_shapes=[
            pltpu.VMEM((chips, 2, columns, 2 * part), bf16),
            pltpu.VMEM((part, width), bf16),
            pltpu.VMEM((chips, columns, 2 * part), bf16),
            pltpu.VMEM((sp_count, tokens, 2 * part), bf16),
            pltpu.VMEM((sp_count, tokens, 2 * part), f32),
            pltpu.VMEM((sp_count, tokens, part), f32),
            pltpu.VMEM((tp_count, 8, tokens), f32),
            pltpu.VMEM((8, tokens), f32),
            pltpu.VMEM((sp_count, 8, tokens), f32),
            pltpu.VMEM((sp_count, 8, tokens), f32),
            dma((2, 3)),
            dma((2, sp_count, chips)),
            dma((2, chips, 2)),
            dma((2, chips)),
            dma((2, sp_count)),
            dma((2, sp_count)),
            dma((tp_count - 1,)),
            dma((tp_count,)),
            dma((3,)),
            dma((sp_count,)),
            dma((3,)),
            dma((sp_count,)),
            dma((2,)),
            dma((sp_count,)),
            dma((sp_count,)),
            dma((5,)),
        ],
        compiler_params=pltpu.CompilerParams(
            collective_id=3, has_side_effects=True, vmem_limit_bytes=VMEM_LIMIT
        ),
        cost_estimate=pl.CostEstimate(
            flops=10**10, bytes_accessed=10**8, transcendentals=0
        ),
        name="expert_gather",
    )(
        scaled_stream,
        upstream,
        stats,
        weight_rows,
        w_gate[0].reshape(piece),
        w_up[0].reshape(piece),
        w_down[0],
    )
    rows_s, rows_u, hidden, active, keep, send_x, send_y, totals = outs

    def swap(block, step):
        route = [(i, i + step if (i // step) % 2 == 0 else i - step) for i in range(sp_count)]
        return lax.ppermute(block, "sp", route)

    got_x = swap(send_x, 1)
    got_y = swap(send_y, 2)

    grad_gate, grad_up, grad_down = pl.pallas_call(
        grads_kernel,
        out_shape=(shape((width, part), f32), shape((width, part), f32), shape((part, width), f32)),
        in_specs=[vmem] * 4,
        out_specs=[anywhere] * 3,
        scratch_shapes=[
            pltpu.VMEM((2, columns, 2 * part), f32),
            pltpu.VMEM((2, part, columns), f32),
            dma((2, 3)),
        ],
        compiler_params=pltpu.CompilerParams(vmem_limit_bytes=VMEM_LIMIT),
        cost_estimate=pl.CostEstimate(
            flops=6 * width * part * tokens * sp_count,
            bytes_accessed=40 * 2**20,
            transcendentals=0,
        ),
        name="weight_grads",
    )(rows_s, rows_u, hidden, active)

    inverse = lax.rsqrt(totals[0] / width + EPSILON)[:, None]
    mean_val = (totals[1] / channels)[:, None]
    variance = (totals[2] / channels)[:, None] - mean_val * mean_val
    inv_std = lax.rsqrt(variance + EPSILON)
    centred = (conv_vals - mean_val) * inv_std
    scaled = centred * ln_gain[None, :]
    mixed_out = jax.nn.silu(scaled).astype(bf16)
    slope = silu_slope(scaled) * ln_gain[None, :]
    rim = -(-(conv_taps.shape[0] - 1) // 8) * 8
    conv_back, grads, mixed = pl.pallas_call(
        functools.partial(return_kernel, width, channels),
        out_shape=(
            shape((tokens + rim, channel_part), f32),
            shape((sp_count, 2, tokens, columns), bf16),
            shape((sp_count, tokens, channel_part), bf16),
        ),
        in_specs=[vmem] * 11 + [anywhere],
        out_specs=[vmem] * 3,
        scratch_shapes=[
            pltpu.VMEM(w_out.shape, bf16),
            pltpu.VMEM((2, 2, tokens, columns), bf16),
            pltpu.VMEM((2, 2, tokens, columns), bf16),
            pltpu.VMEM((chips, tokens, columns), bf16),
            pltpu.VMEM((chips, tokens, columns), bf16),
            pltpu.VMEM((tokens, columns), f32),
            pltpu.VMEM((8, tokens), f32),
            pltpu.VMEM((tp_count, 8, tokens), f32),
            pltpu.VMEM((8, tokens), f32),
            pltpu.VMEM((tp_count, 8, tokens), f32),
            pltpu.VMEM((2, chips, tokens, columns), bf16),
            pltpu.VMEM((rim, channel_part), f32),
            dma((3,)),
            dma((sp_count,)),
            dma((2, 2)),
            dma((2, 2)),
            dma((chips,)),
            dma((chips,)),
            dma((tp_count - 1,)),
            dma((tp_count,)),
            dma((tp_count - 1,)),
            dma((tp_count,)),
            dma((3,)),
            dma((chips,)),
            dma((chips,)),
            dma((chips,)),
            dma((sp_count,)),
            dma((sp_count,)),
            dma((sp_count,)),
            dma((sp_count,)),
            dma((2,)),
            dma((2,)),
        ],
        compiler_params=pltpu.CompilerParams(
            collective_id=4, has_side_effects=True, vmem_limit_bytes=VMEM_LIMIT
        ),
        cost_estimate=pl.CostEstimate(
            flops=10**10, bytes_accessed=10**8, transcendentals=0
        ),
        name="return_path",
    )(
        keep,
        got_x,
        got_y,
        upstream,
        stream,
        norm_gain[None, :],
        inverse,
        mixed_out,
        slope,
        centred,
        inv_std,
        w_out,
    )
    grad_out, value_grad, gate_grad = pl.pallas_call(
        finish_kernel,
        out_shape=(
            shape((channel_part, 2 * columns), f32),
            shape((tokens, channel_part), bf16),
            shape((tokens, channel_part), bf16),
        ),
        in_specs=[vmem] * 6,
        out_specs=[vmem] * 3,
        compiler_params=pltpu.CompilerParams(vmem_limit_bytes=VMEM_LIMIT),
        cost_estimate=pl.CostEstimate(
            flops=10**9, bytes_accessed=10**7, transcendentals=0
        ),
        name="finish",
    )(conv_back, conv_taps, value_in, gate_in, grads, mixed)
    return (grad_gate[None], grad_up[None], grad_down[None], grad_out, value_grad, gate_grad)


def solution(mesh):
    planar = mesh.shape["sp"] == 4 and mesh.shape["tp"] == 2 * mesh.shape["sp"]
    return jax.shard_map(
        fused_device if planar else per_device,
        mesh=mesh,
        in_specs=(
            P("sp", "tp"),
            P("sp", "tp"),
            P("tp"),
            P("sp", None),
            P("sp", None),
            P("sp", None, "tp"),
            P("sp", None, "tp"),
            P("sp", "tp", None),
            P("sp", "tp"),
            P("sp", "tp"),
            P("sp", "tp"),
            P("tp"),
            P(None, "tp"),
            P("tp", None),
        ),
        out_specs=(
            P("sp", None, "tp"),
            P("sp", None, "tp"),
            P("sp", "tp", None),
            P("tp", "sp"),
            P("sp", "tp"),
            P("sp", "tp"),
        ),
        check_vma=False,
    )
```

profile of v0, /device:TPU:19, one launch (start us, length us, event | category | flops | bytes accessed | tf_op | source)
XLA Modules:
  0.0 219.8 jit_solution(9500468393265174055)
XLA Ops:
  0.6 1.1 fusion.2
  1.7 1.7 fusion.1
  3.4 0.7 select_reduce_fusion
  4.2 0.6 stack.19.stat_ref
  4.8 0.6 broadcast_in_dim.24.wrow_ref
  5.4 0.0 copy-start
  5.4 0.0 copy-start.1
  5.4 97.6 %expert_gather.1 = (bf16[4,2,4,256,512]{4,3,2,1,0:T(8,128)(2,1)}, bf16[4,2,4,256,512]{4,3,2,1,0:T(8,128)(2,1)}, bf16[4,256,512]{2,1,0:T(8,128)(2,1)}, bf16[4,256...) custom-call(bf16[256,512]{1,0:T(8,128)(2,1)} %get-tuple-element.43.g, ...), custom_call_target="tpu_custom_call" | custom-call | flops 10000000000 | bytes 100000000 | tf_op jit(solution)/shard_map/expert_gather/pallas_call | solution.py:1005
  103.0 0.4 collective-permute-start
  103.4 1.0 collective-permute-start.1
  104.4 0.8 rsqrt_bitcast_fusion
  105.3 0.8 copy.26.inv_ref
  106.1 0.8 copy.27.invstd_ref
  106.9 0.0 copy-done
  106.9 0.0 copy-done.1
  106.9 1.0 multiply_multiply_fusion
  107.9 15.4 %weight_grads.1 = (f32[4096,256]{1,0:T(8,128)}, f32[4096,256]{1,0:T(8,128)}, f32[256,4096]{1,0:T(8,128)}) custom-call(bf16[4,2,4,256,512]{4,3,2,1,0:T(8,128)(2,1)} %get-tuple-element.23.rows_s, bf16[4,2,4,256,512]{4,3,2,1,0:T(8,128)(2,1)} %get-tuple-element.24.rows_u, bf16[4,256,512]{2,1,0:T(8,128)(2,1)} %get-tuple-element.25.hidden, ...), custom_call_target="tpu_custom_call" | custom-call | flops 6442450944 | bytes 41943040 | tf_op jit(solution)/shard_map/weight_grads/pallas_call | solution.py:1072
  123.3 4.8 %collective-permute-done.got_x = bf16[2,2,256,512]{3,2,1,0:T(8,128)(2,1)S(1)} collective-permute-done((bf16[2,2,256,512]{3,2,1,0:T(8,128)(2,1)}, bf16[2,2,256,512]{3,2,1,0:T(8,128)(2,1)S(1)}, u32[]{:S(2)}, u32[]{:S(2)}) %collective-permute-start) | collective-permute-done | bytes 1048608 | tf_op jit(solution)/shard_map/ppermute | solution.py:1067
  128.1 0.0 copy-start.2
  128.1 0.2 collective-permute-done.1.got_y
  128.2 0.8 copy-done.2
  129.1 0.4 copy-done.3
  129.4 85.8 %return_path.1 = (f32[288,256]{1,0:T(8,128)}, bf16[4,2,256,512]{3,2,1,0:T(8,128)(2,1)}, bf16[4,256,256]{2,1,0:T(8,128)(2,1)}) custom-call(bf16[2,2,2,256,512]{4,3,2,1,0:T(8,128)(2,1)} %get-tuple-element.30.keep, bf16[2,2,256,512]{3,2,1,0:T(8,128)(2,1)} %copy-done.2, bf16[2,2,256,512]{3,2,1,0:T(8,128)(2,1)} %copy-done.3, bf16[256,512]{1,0:T(8,128)(2,1)} %up_ref.3, ...), custom_call_target="tpu_custom_call" | custom-call | flops 10000000000 | bytes 100000000 | tf_op jit(solution)/shard_map/return_path/pallas_call | solution.py:1100
  215.2 4.6 %finish.1 = (f32[256,1024]{1,0:T(8,128)}, bf16[256,256]{1,0:T(8,128)(2,1)}, bf16[256,256]{1,0:T(8,128)(2,1)}) custom-call(f32[288,256]{1,0:T(8,128)} %get-tuple-element.34.conv, f32[31,256]{1,0:T(8,128)} %taps.1, bf16[256,256]{1,0:T(8,128)(2,1)} %value_in.1, bf16[256,256]{1,0:T(8,128)(2,1)} %gate_in.1, bf16[4,2,256,512]{3,2,1,0:T(8,128)(2,1)} %get-tuple-element.35.grads, ...), custom_call_target="tpu_custom_call" | custom-call | flops 1000000000 | bytes 10000000 | tf_op jit(solution)/shard_map/finish/pallas_call | solution.py:1164
  (4 shorter events, 0.0 us)
Async XLA Ops:
  5.4 101.5 %copy-start = (bf16[256,256]{1,0:T(8,128)(2,1)S(1)}, bf16[256,256]{1,0:T(8,128)(2,1)}, u32[]{:S(2)}) copy-start(bf16[256,256]{1,0:T(8,128)(2,1)} %param.24) | copy-start | bytes 393220
  5.4 101.5 %copy-start.1 = (f32[256]{0:T(256)S(1)}, f32[256]{0:T(256)}, u32[]{:S(2)}) copy-start(f32[256]{0:T(256)} %param.25) | copy-start | bytes 3076
  103.0 25.1 %collective-permute-start = (bf16[2,2,256,512]{3,2,1,0:T(8,128)(2,1)}, bf16[2,2,256,512]{3,2,1,0:T(8,128)(2,1)S(1)}, u32[]{:S(2)}, u32[]{:S(2)}) collective-permute-start(bf16[2,2,256,512]{3,2,1,0:T(8,128)(2,1)} %get-tuple-element.31), channel_id=1, source_target_pairs={{0,8},{8,0},{16,24},{24,16},{1,9},{9,1},{17,25},{25,17},{2,10},{10... | collective-permute-start | bytes 3145736 | tf_op jit(solution)/shard_map/ppermute | solution.py:1067
  103.4 24.8 %collective-permute-start.1 = (bf16[2,2,256,512]{3,2,1,0:T(8,128)(2,1)}, bf16[2,2,256,512]{3,2,1,0:T(8,128)(2,1)S(1)}, u32[]{:S(2)}, u32[]{:S(2)}) collective-permute-start(bf16[2,2,256,512]{3,2,1,0:T(8,128)(2,1)} %get-tuple-element.32), channel_id=1, source_target_pairs={{0,16},{8,24},{16,0},{24,8},{1,17},{9,25},{17,1},{25,9},{2,18},{10... | collective-permute-start | bytes 3145736 | tf_op jit(solution)/shard_map/ppermute | solution.py:1067
  128.1 1.0 copy-start.2
  128.2 1.2 copy-start.3
where the time goes:
time: 220 us
  Pallas kernels  203 us (92%)
  other arithmetic  5.33 us (2%)
  waiting for transfers between devices  4.94 us (2%)
  local copies, waits for them, and re-layouts  4.03 us (2%)
    pallas_call x1, Pallas kernels, fused_device(): pl.pallas_call(functools.partial(expert_kernel, width), out_shape=(shape(...  97.6 us
    pallas_call x1, Pallas kernels, fused_device(): pl.pallas_call(functools.partial(return_kernel, width, channels), out_sha...  85.8 us
    pallas_call x1, Pallas kernels, fused_device(): pl.pallas_call(grads_kernel, out_shape=(shape((width, part), f32), shape(...  15.4 us
    ppermute x2, waiting for transfers between devices, swap(): return lax.ppermute(block, 'sp', route)  4.94 us
    pallas_call x1, Pallas kernels, fused_device(): pl.pallas_call(finish_kernel, out_shape=(shape((channel_part, 2 * columns...  4.58 us
  transfers between devices with their start and end apart: 2, of which 2 were waited for; matrix products, arithmetic and copies ran while one was open for 2% of the time, Pallas kernels for 7%

commit v1 on v0

--- a/solution.py
+++ b/solution.py
@@ -255,7 +255,7 @@
     )
 
 
-def greet(devices):
+def signal(devices):
     barrier = pltpu.get_barrier_semaphore()
     for sp_index, tp_index in devices:
         pl.semaphore_signal(
@@ -264,7 +264,10 @@
             device_id={"sp": sp_index, "tp": tp_index},
             device_id_type=MESH_ID,
         )
-    pl.semaphore_wait(barrier, len(devices))
+
+
+def await_signals(count):
+    pl.semaphore_wait(pltpu.get_barrier_semaphore(), count)
 
 
 def places():
@@ -278,8 +281,8 @@
     hops = (
         chip,
         chip + 1 - 2 * (chip % 2),
-        chip + 2 - 4 * (chip // 2),
-        3 - chip,
+        2 - chip // 2,
+        3 - 3 * (chip // 2),
     )
     return sp, tp, chip, core, across, along, corner, hops
 
@@ -312,13 +315,25 @@
 
 def expert_kernel(
     width,
-    gs_ref,
+    stream_ref,
     up_ref,
-    stat_ref,
-    wrow_ref,
+    gain_ref,
+    routes_ref,
+    weights_ref,
+    conv_ref,
     wg_hbm,
     wu_hbm,
     wd_hbm,
+    rows_s_out,
+    rows_u_out,
+    hidden_out,
+    active_out,
+    keep_out,
+    far_x_out,
+    far_y_out,
+    near_x_out,
+    near_y_out,
+    stat_out,
     rows_s,
     rows_u,
     hidden,
@@ -326,7 +341,9 @@
     keep,
     send_x,
     send_y,
-    stat_out,
+    gs_ref,
+    stat_ref,
+    wrow_ref,
     wgu,
     wd,
     mate_w,
@@ -343,6 +360,11 @@
     relay_send,
     mate_send,
     mate_recv,
+    last_send,
+    last_recv,
+    c_send,
+    near_send,
+    near_recv,
     stat_send,
     stat_recv,
     inv_send,
@@ -353,33 +375,68 @@
     mh_send,
     mh_recv,
     local_sems,
+    rows_sems,
+    small_sems,
 ):
     sp, tp, chip, core, across, along, corner, hops = places()
     mate = tp + 1 - 2 * core
     tokens, columns = gs_ref.shape
     part = wd_hbm.shape[0]
-    tp_count = 8
+    sp_count, tp_count = 4, 8
+    row_of = sp // 2
+    col_of = lax.rem(sp, 2)
     peers = [lax.rem(tp + step, tp_count) for step in range(1, tp_count)]
     others = (across, along, corner)
     owns = (gs_ref, up_ref)
     rows = (rows_s, rows_u)
-
+    rows_out = (rows_s_out, rows_u_out)
+
+    signal([(sp, peer) for peer in peers] + [(other, tp) for other in others])
     loads = [
+        pltpu.make_async_copy(up_ref, rows_u.at[sp, core, chip], local_sems.at[3]),
         pltpu.make_async_copy(wg_hbm, wgu.at[:, :, :, pl.ds(0, part)], local_sems.at[0]),
         pltpu.make_async_copy(wu_hbm, wgu.at[:, :, :, pl.ds(part, part)], local_sems.at[1]),
         pltpu.make_async_copy(wd_hbm, wd, local_sems.at[2]),
-        pltpu.make_async_copy(gs_ref, rows_s.at[sp, core, chip], local_sems.at[3]),
-        pltpu.make_async_copy(up_ref, rows_u.at[sp, core, chip], local_sems.at[4]),
     ]
     for load in loads:
         load.start()
-    greet([(sp, peer) for peer in peers] + [(other, tp) for other in others])
+    own_rows = pltpu.make_async_copy(gs_ref, rows_s.at[sp, core, chip], local_sems.at[4])
+
+    gain = gain_ref[...]
+    squares = []
+    for begin in range(0, tokens, 64):
+        block = stream_ref[begin : begin + 64].astype(jnp.float32)
+        gs_ref[begin : begin + 64] = (gain * block).astype(jnp.bfloat16)
+        squares.append(jnp.sum(block * block, axis=1, keepdims=True))
+    conv_vals = conv_ref[...].astype(jnp.float32)
+    stat_ref[...] = jnp.concatenate(
+        [
+            to_row(jnp.concatenate(squares, axis=0)),
+            to_row(jnp.sum(conv_vals, axis=1, keepdims=True)),
+            to_row(jnp.sum(conv_vals * conv_vals, axis=1, keepdims=True)),
+            jnp.zeros((5, tokens), jnp.float32),
+        ],
+        axis=0,
+    )
+    for expert in range(sp_count):
+        row = jnp.sum(
+            jnp.where(routes_ref[...] == expert, weights_ref[...], 0.0), axis=0, keepdims=True
+        )
+        wrow_ref[expert] = jnp.broadcast_to(row, (8, tokens))
+    await_signals(len(peers) + len(others))
+    own_rows.start()
 
     pending = []
+    stores = []
 
     def go(copy):
         copy.start()
         pending.append(copy)
+
+    def store(source, target, sem):
+        copy = pltpu.make_async_copy(source, target, sem)
+        copy.start()
+        stores.append(copy)
 
     for i, peer in enumerate(peers):
         go(remote(stat_ref, stat_in.at[tp], stat_send.at[i], stat_recv.at[tp], sp, peer))
@@ -400,18 +457,39 @@
                 )
             )
 
+    edge = lax.rem(chip + 1, 4) // 2 == 0
+    middle = jnp.logical_not(edge)
+
+    def z_copy(kind, origin, step, send_sem, source=None):
+        slot = rows[kind].at[origin, core, chip]
+        return remote(
+            slot if source is None else source,
+            slot,
+            send_sem,
+            piece_recv.at[kind, origin, chip],
+            sp,
+            2 * hops[step] + core,
+        )
+
+    def pass_copy(kind, origin, send_sem):
+        slot = rows[kind].at[origin, core, hops[2]]
+        return remote(
+            slot,
+            slot,
+            send_sem,
+            piece_recv.at[kind, origin, hops[2]],
+            sp,
+            2 * hops[1] + core,
+        )
+
     for kind in (0, 1):
-        for step in (1, 2, 3):
-            go(
-                remote(
-                    owns[kind],
-                    rows[kind].at[sp, core, chip],
-                    z_send.at[kind, step - 1],
-                    piece_recv.at[kind, sp, chip],
-                    sp,
-                    2 * hops[step] + core,
-                )
-            )
+        for step in (1, 2):
+            go(z_copy(kind, sp, step, z_send.at[kind, step - 1], owns[kind]))
+
+        @pl.when(edge)
+        def _(kind=kind):
+            z_copy(kind, sp, 3, z_send.at[kind, 2], owns[kind]).start()
+
         send_piece(kind, 0, owns[kind])
 
     def await_piece(kind, origin, step):
@@ -447,20 +525,15 @@
                 slot, slot, mate_send.at[kind, origin], mate_recv.at[kind, origin], sp, mate
             )
         )
+        store(slot, rows_out[kind].at[origin, core], rows_sems.at[kind, origin, 0])
 
     def await_share(kind, origin):
         slot = rows[kind].at[origin, 1 - core]
         remote(
             slot, slot, mate_send.at[kind, origin], mate_recv.at[kind, origin], sp, mate
         ).wait_recv()
-
-    for load in loads:
-        load.wait()
-    go(
-        remote(
-            wgu.at[:, 1 - core], mate_w, mw_sems.at[0], mw_sems.at[1], sp, mate
-        )
-    )
+        store(slot, rows_out[kind].at[origin, 1 - core], rows_sems.at[kind, origin, 1])
+
     acc[...] = jnp.zeros(acc.shape, jnp.float32)
     back[...] = jnp.zeros(back.shape, jnp.float32)
     w_in[sp] = wrow_ref[sp]
@@ -490,13 +563,16 @@
 
         lax.fori_loop(0, tp_count, body, 0)
 
-    def backward(origin, half):
-        def body(place, carry):
-            start = pl.multiple_of((2 * place + half) * columns, columns)
-            back[origin] += dot_nt(rows_u[origin, half, place], wd[:, pl.ds(start, columns)])
+    def backward_piece(origin, half, place):
+        start = pl.multiple_of((2 * place + half) * columns, columns)
+        back[origin] += dot_nt(rows_u[origin, half, place], wd[:, pl.ds(start, columns)])
+
+    def backward(origin):
+        def body(index, carry):
+            backward_piece(origin, index // 4, lax.rem(index, 4))
             return carry
 
-        lax.fori_loop(0, 4, body, 0)
+        lax.fori_loop(0, tp_count, body, 0)
 
     chunk = 64
 
@@ -535,6 +611,8 @@
             sp,
             mate,
         ).wait_recv()
+        store(hidden.at[origin], hidden_out.at[origin], small_sems.at[0, origin])
+        store(active.at[origin], active_out.at[origin], small_sems.at[1, origin])
 
         for target, first in ((low, 0), (high, 2)):
 
@@ -548,82 +626,144 @@
 
             lax.fori_loop(0, 2, body, 0)
 
+    def pass_on(kind, origin, send_sem):
+        @pl.when(middle)
+        def _():
+            pass_copy(kind, origin, send_sem).start()
+
     def arrive(kind, step):
         await_piece(kind, sp, step)
+        if step == 2:
+            pass_on(kind, sp, z_send.at[kind, 2])
         send_piece(kind, step, rows[kind].at[sp, core, hops[step]])
 
+    def corner_out(kind):
+        await_piece(kind, corner, 0)
+        go(z_copy(kind, corner, 1, c_send.at[kind, 0]))
+
+        @pl.when(middle)
+        def _():
+            z_copy(kind, corner, 2, c_send.at[kind, 1]).start()
+
+    def corner_in(kind):
+        await_piece(kind, corner, 2)
+        pass_on(kind, corner, c_send.at[kind, 2])
+
+    relay(0, 0)
     arrive(0, 1)
-    relay(0, 0)
+    relay(1, 0)
     arrive(0, 2)
-    relay(1, 0)
+    corner_out(0)
     arrive(0, 3)
-    relay(0, 1)
+    own_rows.wait()
+    for load in loads:
+        load.wait()
     share(0, sp)
+    go(remote(wgu.at[:, 1 - core], mate_w, mw_sems.at[0], mw_sems.at[1], sp, mate))
+    corner_out(1)
     arrive(1, 1)
-    relay(0, 2)
     await_share(0, sp)
     forward(sp)
     arrive(1, 2)
+    corner_in(0)
+    arrive(1, 3)
+    share(1, sp)
     relay(0, 3)
-    for step in (1, 3):
+    for step in (1, 2, 3):
         await_piece(0, across, step)
     share(0, across)
-    for step in (0, 2):
+    for step in (0, 1, 2):
         await_piece(0, along, step)
     share(0, along)
-    arrive(1, 3)
-    relay(1, 1)
-    share(1, sp)
+    await_share(1, sp)
+    backward(sp)
+    corner_in(1)
     await_share(0, across)
     forward(across)
     await_share(0, along)
     forward(along)
-    relay(1, 2)
-    for step in (0, 1, 2, 3):
-        await_piece(0, corner, step)
-    share(0, corner)
-    await_share(1, sp)
-    backward(sp, 0)
-    backward(sp, 1)
-    await_share(0, corner)
-    forward(corner)
-    relay(1, 3)
     for other in others:
         for sems, landing in ((inv_recv, inv_in), (w_recv, w_in)):
             remote(
                 landing.at[other], landing.at[other], inv_send.at[0], sems.at[other], sp, mate
             ).wait_recv()
     activate(sp)
+    relay(1, 3)
     for step in (1, 3):
+        await_piece(0, corner, step)
+    share(0, corner)
+    await_share(0, corner)
+    forward(corner)
+    for step in (1, 2, 3):
         await_piece(1, across, step)
     share(1, across)
-    for step in (0, 2):
+    for step in (0, 1, 2):
         await_piece(1, along, step)
     share(1, along)
     remote(mate_w, mate_w, mw_sems.at[0], mw_sems.at[1], sp, mate).wait_recv()
     await_share(1, across)
-    backward(across, 0)
-    backward(across, 1)
+    backward(across)
     activate(across)
     await_share(1, along)
-    backward(along, 0)
-    backward(along, 1)
+    backward(along)
     activate(along)
-    row_of = sp // 2
-    col_of = lax.rem(sp, 2)
+    spread(across, send_x.at[0], keep.at[1, 1 - col_of])
+    for i in range(2):
+        go(
+            remote(
+                send_x.at[0, i], near_x_out.at[i], near_send.at[0, i], near_recv.at[0, i], across, tp
+            )
+        )
+    store(keep.at[1, 1 - col_of], keep_out.at[1, 1 - col_of], small_sems.at[2, 0])
+    spread(along, keep.at[0, 1 - row_of], send_y.at[0])
+    for i in range(2):
+        go(
+            remote(
+                send_y.at[0, i], near_y_out.at[i], near_send.at[1, i], near_recv.at[1, i], along, tp
+            )
+        )
+    store(keep.at[0, 1 - row_of], keep_out.at[0, 1 - row_of], small_sems.at[2, 1])
     spread(sp, keep.at[0, row_of], keep.at[1, col_of])
-    spread(across, send_x.at[row_of], keep.at[1, 1 - col_of])
-    spread(along, keep.at[0, 1 - row_of], send_y.at[col_of])
+    store(keep.at[0, row_of], keep_out.at[0, row_of], small_sems.at[2, 2])
+    store(keep.at[1, col_of], keep_out.at[1, col_of], small_sems.at[2, 3])
     for step in (0, 1, 2, 3):
-        await_piece(1, corner, step)
-    share(1, corner)
-    backward(corner, core)
-    await_share(1, corner)
-    backward(corner, 1 - core)
+        place = hops[step]
+        if step in (1, 3):
+            await_piece(1, corner, step)
+        slot = rows_u.at[corner, core, place]
+        go(remote(slot, slot, last_send.at[place], last_recv.at[place], sp, mate))
+        backward_piece(corner, core, place)
+    store(rows_u.at[corner, core], rows_u_out.at[corner, core], rows_sems.at[1, corner, 0])
+    for step in (0, 1, 2, 3):
+        place = hops[step]
+        slot = rows_u.at[corner, 1 - core, place]
+        remote(slot, slot, last_send.at[place], last_recv.at[place], sp, mate).wait_recv()
+        backward_piece(corner, 1 - core, place)
+    store(rows_u.at[corner, 1 - core], rows_u_out.at[corner, 1 - core], rows_sems.at[1, corner, 1])
     activate(corner)
-    spread(corner, send_x.at[1 - row_of], send_y.at[1 - col_of])
+    spread(corner, send_x.at[1], send_y.at[1])
+    store(send_x.at[1], far_x_out, small_sems.at[3, 0])
+    store(send_y.at[1], far_y_out, small_sems.at[3, 1])
+    for side, landing in enumerate((near_x_out, near_y_out)):
+        for i in range(2):
+            remote(
+                landing.at[i], landing.at[i], near_send.at[side, i], near_recv.at[side, i], sp, mate
+            ).wait_recv()
+    for copy in stores:
+        copy.wait()
     for copy in pending:
         copy.wait_send()
+    for kind in (0, 1):
+
+        @pl.when(edge)
+        def _(kind=kind):
+            z_copy(kind, sp, 3, z_send.at[kind, 2], owns[kind]).wait_send()
+
+        @pl.when(middle)
+        def _(kind=kind):
+            pass_copy(kind, sp, z_send.at[kind, 2]).wait_send()
+            z_copy(kind, corner, 2, c_send.at[kind, 1]).wait_send()
+            pass_copy(kind, corner, c_send.at[kind, 2]).wait_send()
 
 
 def grads_kernel(rows_s, rows_u, hidden, active, gate_out, up_out, down_out, tall, wide, sems):
@@ -674,27 +814,36 @@
 def return_kernel(
     width,
     channels,
-    keep,
-    got_x,
-    got_y,
+    keep_hbm,
+    far_x_hbm,
+    far_y_hbm,
+    near_x_hbm,
+    near_y_hbm,
     up_ref,
     stream_ref,
     gain_ref,
-    inv_ref,
-    mixed_ref,
-    slope_ref,
-    centred_ref,
-    invstd_ref,
+    stat_ref,
+    conv_ref,
+    ln_ref,
     w_hbm,
     conv_out,
     grads,
     mixed,
     w_out,
+    keep,
+    far,
+    near,
+    mixed_ref,
+    slope_ref,
+    centred_ref,
     turn_out,
     turn_in,
     z_out,
     z_in,
+    over_in,
+    over_sum,
     own_sum,
+    mixed_back,
     note_out,
     note_in,
     tail_out,
@@ -707,6 +856,7 @@
     turn_recv,
     z_send,
     z_recv,
+    over_recv,
     note_send,
     note_recv,
     tail_send,
@@ -730,199 +880,356 @@
     col_of = lax.rem(sp, 2)
     peers = [lax.rem(tp + step, tp_count) for step in range(1, tp_count)]
     others = (across, along, corner)
+    signal([(sp, peer) for peer in peers] + [(other, tp) for other in others])
+    pulls = [
+        pltpu.make_async_copy(source, target, local_sems.at[2 + i])
+        for i, (source, target) in enumerate(
+            (
+                (far_x_hbm, far.at[0]),
+                (far_y_hbm, far.at[1]),
+                (keep_hbm, keep),
+                (near_x_hbm, near.at[0]),
+                (near_y_hbm, near.at[1]),
+            )
+        )
+    ]
+    for pull in pulls:
+        pull.start()
     load = pltpu.make_async_copy(w_hbm, w_out, local_sems.at[0])
     load.start()
+    inverse = to_column(lax.rsqrt(stat_ref[0:1] / width + EPSILON))
+    mean_row = stat_ref[1:2] / channels
+    inv_std = to_column(lax.rsqrt(stat_ref[2:3] / channels - mean_row * mean_row + EPSILON))
+    mean_val = to_column(mean_row)
+    ln_gain = ln_ref[...]
+    for begin in range(0, tokens, 64):
+        end = begin + 64
+        block = (conv_ref[begin:end].astype(jnp.float32) - mean_val[begin:end]) * inv_std[
+            begin:end
+        ]
+        scaled = block * ln_gain
+        logistic = 1.0 / (1.0 + jnp.exp(-scaled))
+        centred_ref[begin:end] = block
+        mixed_ref[begin:end] = (scaled * logistic).astype(jnp.bfloat16)
+        slope_ref[begin:end] = logistic * (1.0 + scaled * (1.0 - logistic)) * ln_gain
+    await_signals(len(peers) + len(others))
     own_mixed = pltpu.make_async_copy(mixed_ref, mixed.at[sp], local_sems.at[1])
     own_mixed.start()
-    greet([(sp, peer) for peer in peers] + [(other, tp) for other in others])
+    for pull in pulls:
+        pull.wait()
     pending = []
 
     def go(copy):
         copy.start()
         pending.append(copy)
 
-    turns = ((0, 1 - row_of, row_of, got_x, along), (1, 1 - col_of, col_of, got_y, across))
-    for i in range(2):
-        for group, far, near, got, target in turns:
-            turn_out[group, i] = (
-                keep[group, far, i].astype(jnp.float32) + got[far, i].astype(jnp.float32)
-            ).astype(jnp.bfloat16)
+    edge = lax.rem(chip + 1, 4) // 2 == 0
+    middle = jnp.logical_not(edge)
+    halves = 2
+    half_rows = tokens // halves
+    spans = [pl.ds(h * half_rows, half_rows) for h in range(halves)]
+
+    def turn_copy(group, i, h):
+        return remote(
+            turn_out.at[group, i, spans[h]],
+            turn_in.at[group, i, spans[h]],
+            turn_send.at[group, i, h],
+            turn_recv.at[group, i, h],
+            (along, across)[group] if isinstance(group, int) else sp,
+            tp,
+        )
+
+    for h in range(halves):
+        for i in range(2):
+            for group, off in ((0, 1 - row_of), (1, 1 - col_of)):
+                turn_out[group, i, spans[h]] = (
+                    keep[group, off, i, spans[h]].astype(jnp.float32)
+                    + far[group, i, spans[h]].astype(jnp.float32)
+                ).astype(jnp.bfloat16)
+                go(turn_copy(group, i, h))
+    for i, other in enumerate(others):
+        go(remote(mixed_ref, mixed.at[sp], mix_send.at[i], mix_recv.at[sp], other, tp))
+
+    def plane_sum(place, h):
+        group, i = place // 2, lax.rem(place, 2)
+        own = row_of + group * (col_of - row_of)
+        remote(
+            turn_in.at[group, i, spans[h]],
+            turn_in.at[group, i, spans[h]],
+            turn_send.at[group, i, h],
+            turn_recv.at[group, i, h],
+            sp,
+            mate,
+        ).wait_recv()
+        return (
+            keep[group, own, i, spans[h]].astype(jnp.float32)
+            + near[group, i, spans[h]].astype(jnp.float32)
+            + turn_in[group, i, spans[h]].astype(jnp.float32)
+        )
+
+    def z_copy(step, h):
+        return remote(
+            z_out.at[step, h],
+            z_in.at[chip, h],
+            z_send.at[step, h],
+            z_recv.at[chip, h],
+            sp,
+            2 * hops[step] + core,
+        )
+
+    def over_copy(h):
+        return remote(
+            z_out.at[2, h], over_in.at[h], z_send.at[2, h], over_recv.at[h], sp, 2 * hops[1] + core
+        )
+
+    def await_z(step, h):
+        slot = z_in.at[hops[step], h]
+        remote(slot, slot, z_send.at[0, h], z_recv.at[hops[step], h], sp, mate).wait_recv()
+
+    def reduce_out(h):
+        summed = plane_sum(hops[2], h)
+
+        @pl.when(edge)
+        def _():
+            z_out[2, h] = summed.astype(jnp.bfloat16)
+            over_copy(h).start()
+
+        @pl.when(middle)
+        def _():
+            over_sum[h] = summed
+
+        for step in (3, 1):
+            z_out[step, h] = plane_sum(hops[step], h).astype(jnp.bfloat16)
+            go(z_copy(step, h))
+        own_sum[spans[h]] = plane_sum(chip, h)
+
+    def reduce_over(h):
+        @pl.when(middle)
+        def _():
+            slot = over_in.at[h]
+            remote(slot, slot, z_send.at[2, h], over_recv.at[h], sp, mate).wait_recv()
+            z_out[2, h] = (over_sum[h] + over_in[h].astype(jnp.float32)).astype(jnp.bfloat16)
+            z_copy(2, h).start()
+
+    gain = gain_ref[...]
+    inner_rows = []
+
+    def reduce_in(h):
+        for step in (1, 2):
+            await_z(step, h)
+        total = (
+            own_sum[spans[h]]
+            + z_in[hops[1], h].astype(jnp.float32)
+            + z_in[hops[2], h].astype(jnp.float32)
+        )
+        own_sum[spans[h]] = total
+
+        @pl.when(edge)
+        def _():
+            await_z(3, h)
+            own_sum[spans[h]] += z_in[hops[3], h].astype(jnp.float32)
+
+        gained = gain * own_sum[spans[h]]
+        own_sum[spans[h]] = gained
+        row = to_row(
+            jnp.sum(gained * stream_ref[spans[h]].astype(jnp.float32), axis=1, keepdims=True)
+        )
+        inner_rows.append(row)
+        note_out[h] = jnp.broadcast_to(row, note_out.shape[1:])
+        for i, peer in enumerate(peers):
             go(
                 remote(
-                    turn_out.at[group, i],
-                    turn_in.at[group, i],
-                    turn_send.at[group, i],
-                    turn_recv.at[group, i],
-                    target,
-                    tp,
+                    note_out.at[h], note_in.at[tp, h], note_send.at[i, h], note_recv.at[tp, h], sp, peer
                 )
             )
-    for i, other in enumerate(others):
-        go(remote(mixed_ref, mixed.at[sp], mix_send.at[i], mix_recv.at[sp], other, tp))
-    for i in range(2):
-        for group, far, near, got, target in turns:
-            place = 2 * group + i
-            remote(
-                turn_in.at[group, i],
-                turn_in.at[group, i],
-                turn_send.at[group, i],
-                turn_recv.at[group, i],
-                target,
-                tp,
-            ).wait_recv()
-            summed = (
-                keep[group, near, i].astype(jnp.float32)
-                + got[near, i].astype(jnp.float32)
-                + turn_in[group, i].astype(jnp.float32)
-            )
-
-            @pl.when(chip == place)
-            def _(summed=summed):
-                own_sum[...] = summed
-
-            @pl.when(chip != place)
-            def _(summed=summed, place=place):
-                z_out[place] = summed.astype(jnp.bfloat16)
-                remote(
-                    z_out.at[place],
-                    z_in.at[chip],
-                    z_send.at[place],
-                    z_recv.at[chip],
-                    sp,
-                    2 * place + core,
-                ).start()
-
-    for step in (1, 2, 3):
+
+    def full_slot(place, h, half=None):
+        return full.at[core if half is None else half, place, spans[h]]
+
+    def full_copy(step, h):
+        slot = full_slot(chip, h)
+        return remote(
+            slot, slot, full_send.at[step - 1, h], full_recv.at[chip, h], sp, 2 * hops[step] + core
+        )
+
+    def full_pass(h):
+        slot = full_slot(hops[2], h)
+        return remote(
+            slot, slot, full_send.at[2, h], full_recv.at[hops[2], h], sp, 2 * hops[1] + core
+        )
+
+    def gather_out(h):
+        row = inner_rows[h]
+        for peer in peers:
+            slot = note_in.at[peer, h]
+            remote(slot, slot, note_send.at[0, h], note_recv.at[peer, h], sp, peer).wait_recv()
+            row = row + note_in[peer, h, 0:1]
+        scale = inverse[h * half_rows : (h + 1) * half_rows]
+        factor = scale * scale * to_column(row) / width
+        full[core, chip, spans[h]] = (
+            up_ref[spans[h]].astype(jnp.float32)
+            + own_sum[spans[h]]
+            - stream_ref[spans[h]].astype(jnp.float32) * factor
+        ).astype(jnp.bfloat16)
+        for step in (1, 2):
+            go(full_copy(step, h))
+
+        @pl.when(edge)
+        def _():
+            full_copy(3, h).start()
+
+    def mate_copy(place, h, half=None):
+        slot = full_slot(place, h, half)
+        return remote(slot, slot, mate_send.at[place, h], mate_recv.at[place, h], sp, mate)
+
+    def grad_copy(place, h):
+        return remote(
+            full_slot(place, h),
+            grads.at[sp, core, spans[h]],
+            grad_send.at[place, h],
+            grad_recv.at[sp, h],
+            place,
+            tp,
+        )
+
+    def mixed_term(half, place, h):
+        start = pl.multiple_of((2 * place + half) * columns, columns)
+        return dot_nt(full[half, place, spans[h]], w_out[:, pl.ds(start, columns)])
+
+    def fan(step, h):
         place = hops[step]
-        remote(
-            z_out.at[place], z_in.at[place], z_send.at[place], z_recv.at[place], sp, mate
-        ).wait()
-
-    gain = gain_ref[...]
-    chunk = 64
-    for begin in range(0, tokens, chunk):
-        end = begin + chunk
-        own_sum[begin:end] = gain * (
-            own_sum[begin:end]
-            + z_in[hops[1], begin:end].astype(jnp.float32)
-            + z_in[hops[2], begin:end].astype(jnp.float32)
-            + z_in[hops[3], begin:end].astype(jnp.float32)
-        )
-    inner = jnp.sum(own_sum[...] * stream_ref[...].astype(jnp.float32), axis=1, keepdims=True)
-    inner_row = to_row(inner)
-    note_out[...] = jnp.broadcast_to(inner_row, note_out.shape)
-    for i, peer in enumerate(peers):
-        go(remote(note_out, note_in.at[tp], note_send.at[i], note_recv.at[tp], sp, peer))
-    for peer in peers:
-        remote(
-            note_in.at[peer], note_in.at[peer], note_send.at[0], note_recv.at[peer], sp, peer
-        ).wait_recv()
-        inner_row = inner_row + note_in[peer, 0:1]
-    inverse = inv_ref[...]
-    factor = inverse * inverse * to_column(inner_row) / width
-    for begin in range(0, tokens, chunk):
-        end = begin + chunk
-        full[core, chip, begin:end] = (
-            up_ref[begin:end].astype(jnp.float32)
-            + own_sum[begin:end]
-            - stream_ref[begin:end].astype(jnp.float32) * factor[begin:end]
-        ).astype(jnp.bfloat16)
-    slot = full.at[core, chip]
-    for step in (1, 2, 3):
-        go(
-            remote(
-                slot,
-                slot,
-                full_send.at[step - 1],
-                full_recv.at[chip],
-                sp,
-                2 * hops[step] + core,
-            )
-        )
-
-    def fan(step):
-        place = hops[step]
-        slot = full.at[core, place]
         if step > 0:
-            remote(slot, slot, full_send.at[0], full_recv.at[place], sp, mate).wait_recv()
-        remote(slot, slot, mate_send.at[place], mate_recv.at[place], sp, mate).start()
+            slot = full_slot(place, h)
+            remote(slot, slot, full_send.at[0, h], full_recv.at[place, h], sp, mate).wait_recv()
+        if step == 2:
+
+            @pl.when(middle)
+            def _():
+                full_pass(h).start()
+
+        mate_copy(place, h).start()
 
         @pl.when(place != sp)
         def _():
-            remote(
-                slot, grads.at[sp, core], grad_send.at[place], grad_recv.at[sp], place, tp
-            ).start()
-
-    load.wait()
-
-    def mixed_term(half, place):
-        start = pl.multiple_of((2 * place + half) * columns, columns)
-        return dot_nt(full[half, place], w_out[:, pl.ds(start, columns)])
-
-    mixed_back = None
-    for step in range(4):
-        fan(step)
-        term = mixed_term(core, hops[step])
-        mixed_back = term if mixed_back is None else mixed_back + term
-    for step in range(4):
-        place = hops[step]
-        slot = full.at[1 - core, place]
-        remote(slot, slot, mate_send.at[place], mate_recv.at[place], sp, mate).wait_recv()
-        mixed_back = mixed_back + mixed_term(1 - core, place)
-    norm_in = mixed_back * slope_ref[...]
-    centred = centred_ref[...]
-    sums = jnp.concatenate(
-        [
-            to_row(jnp.sum(norm_in, axis=1, keepdims=True)),
-            to_row(jnp.sum(norm_in * centred, axis=1, keepdims=True)),
-            jnp.zeros((6, tokens), jnp.float32),
-        ],
-        axis=0,
-    )
-    tail_out[...] = sums
-    for i, peer in enumerate(peers):
-        go(remote(tail_out, tail_in.at[tp], tail_send.at[i], tail_recv.at[tp], sp, peer))
-    for peer in peers:
-        remote(
-            tail_in.at[peer], tail_in.at[peer], tail_send.at[0], tail_recv.at[peer], sp, peer
-        ).wait_recv()
-        sums = sums + tail_in[peer]
-    conv_out[0:tokens] = invstd_ref[...] * (
-        norm_in - to_column(sums[0:1]) / channels - centred * (to_column(sums[1:2]) / channels)
-    )
+            grad_copy(place, h).start()
+
+        term = mixed_term(core, place, h)
+        if step == 0:
+            mixed_back[spans[h]] = term
+        else:
+            mixed_back[spans[h]] += term
+
+    tails = []
+
+    def norm_out(h):
+        total = mixed_back[spans[h]]
+        for step in range(4):
+            place = hops[step]
+            mate_copy(place, h, 1 - core).wait_recv()
+            total = total + mixed_term(1 - core, place, h)
+        norm_in = total * slope_ref[spans[h]]
+        mixed_back[spans[h]] = norm_in
+        sums = jnp.concatenate(
+            [
+                to_row(jnp.sum(norm_in, axis=1, keepdims=True)),
+                to_row(jnp.sum(norm_in * centred_ref[spans[h]], axis=1, keepdims=True)),
+                jnp.zeros((6, half_rows), jnp.float32),
+            ],
+            axis=0,
+        )
+        tails.append(sums)
+        tail_out[h] = sums
+        for i, peer in enumerate(peers):
+            go(
+                remote(
+                    tail_out.at[h], tail_in.at[tp, h], tail_send.at[i, h], tail_recv.at[tp, h], sp, peer
+                )
+            )
+
+    def norm_back(h):
+        sums = tails[h]
+        for peer in peers:
+            slot = tail_in.at[peer, h]
+            remote(slot, slot, tail_send.at[0, h], tail_recv.at[peer, h], sp, peer).wait_recv()
+            sums = sums + tail_in[peer, h]
+        conv_out[spans[h]] = inv_std[h * half_rows : (h + 1) * half_rows] * (
+            mixed_back[spans[h]]
+            - to_column(sums[0:1]) / channels
+            - centred_ref[spans[h]] * (to_column(sums[1:2]) / channels)
+        )
+
+    def grads_in(h):
+        for other in others:
+            slot = grads.at[other, core, spans[h]]
+            remote(slot, slot, grad_send.at[0, h], grad_recv.at[other, h], other, tp).wait_recv()
+            go(
+                remote(
+                    slot, slot, gmate_send.at[other, h], gmate_recv.at[other, h], sp, mate
+                )
+            )
+
     rim = rim_in.shape[0]
     before = lax.rem(sp + 3, 4)
+    reduce_out(0)
+    reduce_out(1)
+    reduce_over(0)
+    reduce_over(1)
+    reduce_in(0)
+    gather_out(0)
+    reduce_in(1)
+    load.wait()
+    fan(0, 0)
+    fan(1, 0)
+    gather_out(1)
+    fan(2, 0)
+    fan(3, 0)
+    fan(0, 1)
+    fan(1, 1)
+    norm_out(0)
+    fan(2, 1)
+    norm_back(0)
     go(
         remote(
             conv_out.at[pl.ds(0, rim)], rim_in, rim_sems.at[0], rim_sems.at[1], before, tp
         )
     )
-    for half in range(2):
-        grads[sp, half] = full[half, sp]
-    for other in others:
-        slot = grads.at[other, core]
-        remote(slot, slot, grad_send.at[0], grad_recv.at[other], other, tp).wait_recv()
-        go(remote(slot, slot, gmate_send.at[other], gmate_recv.at[other], sp, mate))
+    grads_in(0)
     own_mixed.wait()
     for other in others:
         slot = mixed.at[other]
         remote(slot, slot, mix_send.at[0], mix_recv.at[other], other, tp).wait_recv()
-    for other in others:
-        slot = grads.at[other, 1 - core]
-        remote(slot, slot, gmate_send.at[other], gmate_recv.at[other], sp, mate).wait_recv()
+    fan(3, 1)
+    norm_out(1)
+    for half in range(2):
+        grads[sp, half] = full[half, sp]
+    grads_in(1)
+    norm_back(1)
     remote(rim_in, rim_in, rim_sems.at[0], rim_sems.at[1], before, tp).wait_recv()
     last = (sp < 3).astype(jnp.float32)
     conv_out[tokens : tokens + rim] = rim_in[...] * last
-    for step in range(4):
-        place = hops[step]
-        slot = full.at[core, place]
-        remote(slot, slot, mate_send.at[place], mate_recv.at[place], sp, mate).wait_send()
-
-        @pl.when(place != sp)
-        def _(slot=slot, place=place):
+    for h in range(halves):
+        for other in others:
+            slot = grads.at[other, 1 - core, spans[h]]
             remote(
-                slot, grads.at[sp, core], grad_send.at[place], grad_recv.at[sp], place, tp
-            ).wait_send()
+                slot, slot, gmate_send.at[other, h], gmate_recv.at[other, h], sp, mate
+            ).wait_recv()
+        for step in range(4):
+            place = hops[step]
+            mate_copy(place, h).wait_send()
+
+            @pl.when(place != sp)
+            def _(place=place, h=h):
+                grad_copy(place, h).wait_send()
+
+        @pl.when(edge)
+        def _(h=h):
+            over_copy(h).wait_send()
+            full_copy(3, h).wait_send()
+
+        @pl.when(middle)
+        def _(h=h):
+            z_copy(2, h).wait_send()
+            full_pass(h).wait_send()
 
     for copy in pending:
         copy.wait_send()
@@ -983,23 +1290,6 @@
     dma = pltpu.SemaphoreType.DMA
     shape = jax.ShapeDtypeStruct
 
-    residual = stream.astype(f32)
-    scaled_stream = (norm_gain[None, :] * residual).astype(bf16)
-    conv_vals = conv_pre.astype(f32)
-    stats = jnp.stack(
-        [
-            jnp.sum(residual * residual, axis=1),
-            jnp.sum(conv_vals, axis=1),
-            jnp.sum(conv_vals * conv_vals, axis=1),
-        ]
-        + [jnp.zeros((tokens,), f32)] * 5,
-        axis=0,
-    )
-    expert_ids = jnp.arange(sp_count, dtype=jnp.int32)
-    weights = jnp.sum(
-        jnp.where(routes[None] == expert_ids[:, None, None], route_weights[None], 0.0), axis=2
-    )
-    weight_rows = jnp.broadcast_to(weights[:, None, :], (sp_count, 8, tokens))
     piece = (chips, 2, columns, part)
     rows_shape = (sp_count, 2, chips, tokens, columns)
     outs = pl.pallas_call(
@@ -1010,13 +1300,25 @@
             shape((sp_count, tokens, 2 * part), bf16),
             shape((sp_count, tokens, part), bf16),
             shape((2, 2, 2, tokens, columns), bf16),
-            shape((2, 2, tokens, columns), bf16),
-            shape((2, 2, tokens, columns), bf16),
+            shape((2, tokens, columns), bf16),
+            shape((2, tokens, columns), bf16),
+            shape((2, tokens, columns), bf16),
+            shape((2, tokens, columns), bf16),
             shape((8, tokens), f32),
         ),
-        in_specs=[vmem, vmem, vmem, vmem, anywhere, anywhere, anywhere],
-        out_specs=[vmem] * 8,
+        in_specs=[vmem] * 6 + [anywhere] * 3,
+        out_specs=[anywhere] * 9 + [vmem],
         scratch_shapes=[
+            pltpu.VMEM(rows_shape, bf16),
+            pltpu.VMEM(rows_shape, bf16),
+            pltpu.VMEM((sp_count, tokens, 2 * part), bf16),
+            pltpu.VMEM((sp_count, tokens, part), bf16),
+            pltpu.VMEM((2, 2, 2, tokens, columns), bf16),
+            pltpu.VMEM((2, 2, tokens, columns), bf16),
+            pltpu.VMEM((2, 2, tokens, columns), bf16),
+            pltpu.VMEM((tokens, columns), bf16),
+            pltpu.VMEM((8, tokens), f32),
+            pltpu.VMEM((sp_count, 8, tokens), f32),
             pltpu.VMEM((chips, 2, columns, 2 * part), bf16),
             pltpu.VMEM((part, width), bf16),
             pltpu.VMEM((chips, columns, 2 * part), bf16),
@@ -1033,6 +1335,11 @@
             dma((2, chips)),
             dma((2, sp_count)),
             dma((2, sp_count)),
+            dma((chips,)),
+            dma((chips,)),
+            dma((2, 3)),
+            dma((2, 2)),
+            dma((2, 2)),
             dma((tp_count - 1,)),
             dma((tp_count,)),
             dma((3,)),
@@ -1043,6 +1350,8 @@
             dma((sp_count,)),
             dma((sp_count,)),
             dma((5,)),
+            dma((2, sp_count, 2)),
+            dma((4, sp_count)),
         ],
         compiler_params=pltpu.CompilerParams(
             collective_id=3, has_side_effects=True, vmem_limit_bytes=VMEM_LIMIT
@@ -1052,22 +1361,24 @@
         ),
         name="expert_gather",
     )(
-        scaled_stream,
+        stream,
         upstream,
-        stats,
-        weight_rows,
+        norm_gain[None, :],
+        routes.T,
+        route_weights.T,
+        conv_pre,
         w_gate[0].reshape(piece),
         w_up[0].reshape(piece),
         w_down[0],
     )
-    rows_s, rows_u, hidden, active, keep, send_x, send_y, totals = outs
+    rows_s, rows_u, hidden, active, keep, far_x, far_y, near_x, near_y, totals = outs
 
     def swap(block, step):
         route = [(i, i + step if (i // step) % 2 == 0 else i - step) for i in range(sp_count)]
         return lax.ppermute(block, "sp", route)
 
-    got_x = swap(send_x, 1)
-    got_y = swap(send_y, 2)
+    got_x = swap(far_x, 1)
+    got_y = swap(far_y, 2)
 
     grad_gate, grad_up, grad_down = pl.pallas_call(
         grads_kernel,
@@ -1088,14 +1399,6 @@
         name="weight_grads",
     )(rows_s, rows_u, hidden, active)
 
-    inverse = lax.rsqrt(totals[0] / width + EPSILON)[:, None]
-    mean_val = (totals[1] / channels)[:, None]
-    variance = (totals[2] / channels)[:, None] - mean_val * mean_val
-    inv_std = lax.rsqrt(variance + EPSILON)
-    centred = (conv_vals - mean_val) * inv_std
-    scaled = centred * ln_gain[None, :]
-    mixed_out = jax.nn.silu(scaled).astype(bf16)
-    slope = silu_slope(scaled) * ln_gain[None, :]
     rim = -(-(conv_taps.shape[0] - 1) // 8) * 8
     conv_back, grads, mixed = pl.pallas_call(
         functools.partial(return_kernel, width, channels),
@@ -1104,41 +1407,51 @@
             shape((sp_count, 2, tokens, columns), bf16),
             shape((sp_count, tokens, channel_part), bf16),
         ),
-        in_specs=[vmem] * 11 + [anywhere],
+        in_specs=[anywhere] * 5 + [vmem] * 6 + [anywhere],
         out_specs=[vmem] * 3,
         scratch_shapes=[
             pltpu.VMEM(w_out.shape, bf16),
+            pltpu.VMEM((2, 2, 2, tokens, columns), bf16),
             pltpu.VMEM((2, 2, tokens, columns), bf16),
             pltpu.VMEM((2, 2, tokens, columns), bf16),
-            pltpu.VMEM((chips, tokens, columns), bf16),
-            pltpu.VMEM((chips, tokens, columns), bf16),
+            pltpu.VMEM((tokens, channel_part), bf16),
+            pltpu.VMEM((tokens, channel_part), f32),
+            pltpu.VMEM((tokens, channel_part), f32),
+            pltpu.VMEM((2, 2, tokens, columns), bf16),
+            pltpu.VMEM((2, 2, tokens, columns), bf16),
+            pltpu.VMEM((chips, 2, tokens // 2, columns), bf16),
+            pltpu.VMEM((chips, 2, tokens // 2, columns), bf16),
+            pltpu.VMEM((2, tokens // 2, columns), bf16),
+            pltpu.VMEM((2, tokens // 2, columns), f32),
             pltpu.VMEM((tokens, columns), f32),
-            pltpu.VMEM((8, tokens), f32),
-            pltpu.VMEM((tp_count, 8, tokens), f32),
-            pltpu.VMEM((8, tokens), f32),
-            pltpu.VMEM((tp_count, 8, tokens), f32),
+            pltpu.VMEM((tokens, channel_part), f32),
+            pltpu.VMEM((2, 8, tokens // 2), f32),
+            pltpu.VMEM((tp_count, 2, 8, tokens // 2), f32),
+            pltpu.VMEM((2, 8, tokens // 2), f32),
+            pltpu.VMEM((tp_count, 2, 8, tokens // 2), f32),
             pltpu.VMEM((2, chips, tokens, columns), bf16),
             pltpu.VMEM((rim, channel_part), f32),
             dma((3,)),
             dma((sp_count,)),
-            dma((2, 2)),
-            dma((2, 2)),
-            dma((chips,)),
-            dma((chips,)),
-            dma((tp_count - 1,)),
-            dma((tp_count,)),
-            dma((tp_count - 1,)),
-            dma((tp_count,)),
-            dma((3,)),
-            dma((chips,)),
-            dma((chips,)),
-            dma((chips,)),
-            dma((sp_count,)),
-            dma((sp_count,)),
-            dma((sp_count,)),
-            dma((sp_count,)),
+            dma((2, 2, 2)),
+            dma((2, 2, 2)),
+            dma((chips, 2)),
+            dma((chips, 2)),
             dma((2,)),
+            dma((tp_count - 1, 2)),
+            dma((tp_count, 2)),
+            dma((tp_count - 1, 2)),
+            dma((tp_count, 2)),
+            dma((3, 2)),
+            dma((chips, 2)),
+            dma((chips, 2)),
+            dma((chips, 2)),
+            dma((sp_count, 2)),
+            dma((sp_count, 2)),
+            dma((sp_count, 2)),
+            dma((sp_count, 2)),
             dma((2,)),
+            dma((7,)),
         ],
         compiler_params=pltpu.CompilerParams(
             collective_id=4, has_side_effects=True, vmem_limit_bytes=VMEM_LIMIT
@@ -1151,14 +1464,14 @@
         keep,
         got_x,
         got_y,
+        near_x,
+        near_y,
         upstream,
         stream,
         norm_gain[None, :],
-        inverse,
-        mixed_out,
-        slope,
-        centred,
-        inv_std,
+        totals,
+        conv_pre,
+        ln_gain[None, :],
         w_out,
     )
     grad_out, value_grad, gate_grad = pl.pallas_call(

time: 220 us -> 195 us (0.89)
  the two profiles are of different devices: /device:TPU:19 before, /device:TPU:0 now
where the time goes in v1:
time: 195 us; the launch traced here: 194 us
  Pallas kernels  191 us (98%)
    pallas_call x1, Pallas kernels, fused_device(): pl.pallas_call(functools.partial(expert_kernel, width), out_shape=(shape(...  105 us
    pallas_call x1, Pallas kernels, fused_device(): pl.pallas_call(functools.partial(return_kernel, width, channels), out_sha...  65.9 us
    pallas_call x1, Pallas kernels, fused_device(): pl.pallas_call(grads_kernel, out_shape=(shape((width, part), f32), shape(...  15.4 us
    pallas_call x1, Pallas kernels, fused_device(): pl.pallas_call(finish_kernel, out_shape=(shape((channel_part, 2 * columns...  4.58 us
  transfers between devices with their start and end apart: 2, of which 0 were waited for; matrix products, arithmetic and copies ran while one was open for 0% of the time, Pallas kernels for 8%

profile of v1, /device:TPU:0, one launch (start us, length us, event | category | flops | bytes accessed | tf_op | source)
XLA Modules:
  0.0 193.7 jit_solution(10842713387025754707)
XLA Ops:
  0.6 104.9 %expert_gather.1 = (bf16[4,2,4,256,512]{4,3,2,1,0:T(8,128)(2,1)}, bf16[4,2,4,256,512]{4,3,2,1,0:T(8,128)(2,1)}, bf16[4,256,512]{2,1,0:T(8,128)(2,1)}, bf16[4,256...) custom-call(bf16[256,512]{1,0:T(8,128)(2,1)} %stream_ref.3, ...), custom_call_target="tpu_custom_call" | custom-call | flops 10000000000 | bytes 100000000 | tf_op jit(solution)/shard_map/expert_gather/pallas_call | solution.py:1295
  105.6 0.6 collective-permute-start
  106.1 0.6 collective-permute-start.1
  106.8 15.4 %weight_grads.1 = (f32[4096,256]{1,0:T(8,128)}, f32[4096,256]{1,0:T(8,128)}, f32[256,4096]{1,0:T(8,128)}) custom-call(bf16[4,2,4,256,512]{4,3,2,1,0:T(8,128)(2,1)} %get-tuple-element.25.rows_s, bf16[4,2,4,256,512]{4,3,2,1,0:T(8,128)(2,1)} %get-tuple-element.26.rows_u, bf16[4,256,512]{2,1,0:T(8,128)(2,1)} %get-tuple-element.27.hidden, ...), custom_call_target="tpu_custom_call" | custom-call | flops 6442450944 | bytes 41943040 | tf_op jit(solution)/shard_map/weight_grads/pallas_call | solution.py:1383
  122.2 0.0 collective-permute-done.far_x_hbm
  122.2 0.0 copy-start
  122.2 0.0 collective-permute-done.1.far_y_hbm
  122.2 0.0 copy-start.1
  122.2 0.8 copy-done
  123.0 0.2 copy-done.1
  123.2 65.9 %return_path.1 = (f32[288,256]{1,0:T(8,128)}, bf16[4,2,256,512]{3,2,1,0:T(8,128)(2,1)}, bf16[4,256,256]{2,1,0:T(8,128)(2,1)}) custom-call(bf16[2,2,2,256,512]{4,3,2,1,0:T(8,128)(2,1)} %get-tuple-element.32.keep_hbm, bf16[2,256,512]{2,1,0:T(8,128)(2,1)} %copy-done, bf16[2,256,512]{2,1,0:T(8,128)(2,1)} %copy-done.1, ...), custom_call_target="tpu_custom_call" | custom-call | flops 10000000000 | bytes 100000000 | tf_op jit(solution)/shard_map/return_path/pallas_call | solution.py:1403
  189.1 4.6 %finish.1 = (f32[256,1024]{1,0:T(8,128)}, bf16[256,256]{1,0:T(8,128)(2,1)}, bf16[256,256]{1,0:T(8,128)(2,1)}) custom-call(f32[288,256]{1,0:T(8,128)} %get-tuple-element.38.conv, f32[31,256]{1,0:T(8,128)} %taps.1, bf16[256,256]{1,0:T(8,128)(2,1)} %value_in.1, bf16[256,256]{1,0:T(8,128)(2,1)} %gate_in.1, bf16[4,2,256,512]{3,2,1,0:T(8,128)(2,1)} %get-tuple-element.39.grads, ...), custom_call_target="tpu_custom_call" | custom-call | flops 1000000000 | bytes 10000000 | tf_op jit(solution)/shard_map/finish/pallas_call | solution.py:1477
Async XLA Ops:
  105.6 16.6 %collective-permute-start = (bf16[2,256,512]{2,1,0:T(8,128)(2,1)}, bf16[2,256,512]{2,1,0:T(8,128)(2,1)S(1)}, u32[]{:S(2)}, u32[]{:S(2)}) collective-permute-start(bf16[2,256,512]{2,1,0:T(8,128)(2,1)} %get-tuple-element.33), channel_id=1, source_target_pairs={{0,8},{8,0},{16,24},{24,16},{1,9},{9,1},{17,25},{25,17},{2,10},{10... | collective-permute-start | bytes 1572872 | tf_op jit(solution)/shard_map/ppermute | solution.py:1378
  106.1 16.1 %collective-permute-start.1 = (bf16[2,256,512]{2,1,0:T(8,128)(2,1)}, bf16[2,256,512]{2,1,0:T(8,128)(2,1)S(1)}, u32[]{:S(2)}, u32[]{:S(2)}) collective-permute-start(bf16[2,256,512]{2,1,0:T(8,128)(2,1)} %get-tuple-element.34), channel_id=1, source_target_pairs={{0,16},{8,24},{16,0},{24,8},{1,17},{9,25},{17,1},{25,9},{2,18},{10... | collective-permute-start | bytes 1572872 | tf_op jit(solution)/shard_map/ppermute | solution.py:1378
  122.2 0.8 copy-start
  122.2 0.9 copy-start.1

commit v2 on v1

--- a/solution.py
+++ b/solution.py
@@ -313,27 +313,27 @@
     )
 
 
-def expert_kernel(
+def step_kernel(
     width,
+    channels,
     stream_ref,
     up_ref,
     gain_ref,
     routes_ref,
     weights_ref,
     conv_ref,
+    ln_ref,
     wg_hbm,
     wu_hbm,
     wd_hbm,
+    w_hbm,
     rows_s_out,
     rows_u_out,
     hidden_out,
     active_out,
-    keep_out,
-    far_x_out,
-    far_y_out,
-    near_x_out,
-    near_y_out,
-    stat_out,
+    conv_out,
+    grads,
+    mixed,
     rows_s,
     rows_u,
     hidden,
@@ -341,8 +341,11 @@
     keep,
     send_x,
     send_y,
+    near,
+    far,
     gs_ref,
     stat_ref,
+    stat_out,
     wrow_ref,
     wgu,
     wd,
@@ -354,6 +357,24 @@
     inv_out,
     inv_in,
     w_in,
+    w_out,
+    mixed_ref,
+    slope_ref,
+    centred_ref,
+    turn_out,
+    turn_in,
+    z_out,
+    z_in,
+    over_in,
+    over_sum,
+    own_sum,
+    mixed_back,
+    note_out,
+    note_in,
+    tail_out,
+    tail_in,
+    full,
+    rim_in,
     z_send,
     piece_recv,
     xy_send,
@@ -365,6 +386,8 @@
     c_send,
     near_send,
     near_recv,
+    far_send,
+    far_recv,
     stat_send,
     stat_recv,
     inv_send,
@@ -377,6 +400,26 @@
     local_sems,
     rows_sems,
     small_sems,
+    mix_send,
+    mix_recv,
+    turn_send,
+    turn_recv,
+    r_send,
+    r_recv,
+    over_recv,
+    note_send,
+    note_recv,
+    tail_send,
+    tail_recv,
+    full_send,
+    full_recv,
+    fm_send,
+    fm_recv,
+    grad_send,
+    grad_recv,
+    gmate_send,
+    gmate_recv,
+    rim_sems,
 ):
     sp, tp, chip, core, across, along, corner, hops = places()
     mate = tp + 1 - 2 * core
@@ -400,6 +443,8 @@
     ]
     for load in loads:
         load.start()
+    out_load = pltpu.make_async_copy(w_hbm, w_out, local_sems.at[5])
+    out_load.start()
     own_rows = pltpu.make_async_copy(gs_ref, rows_s.at[sp, core, chip], local_sems.at[4])
 
     gain = gain_ref[...]
@@ -443,8 +488,7 @@
     for i, other in enumerate(others):
         go(remote(wrow_ref.at[other], w_in.at[sp], w_send.at[i], w_recv.at[sp], other, tp))
 
-    def send_piece(kind, step, source):
-        place = hops[step]
+    def send_piece(kind, step, source, place):
         for way, target in enumerate((across, along)):
             go(
                 remote(
@@ -490,7 +534,7 @@
         def _(kind=kind):
             z_copy(kind, sp, 3, z_send.at[kind, 2], owns[kind]).start()
 
-        send_piece(kind, 0, owns[kind])
+        send_piece(kind, 0, owns[kind], chip)
 
     def await_piece(kind, origin, step):
         slot = rows[kind].at[origin, core, hops[step]]
@@ -545,6 +589,9 @@
         ).wait_recv()
         total = total + stat_in[peer]
     stat_out[...] = total
+    halves = 2
+    half_rows = tokens // halves
+    spans = [pl.ds(h * half_rows, half_rows) for h in range(halves)]
     inverse_row = lax.rsqrt(total[0:1] / width + EPSILON)
     inv_out[...] = jnp.broadcast_to(inverse_row, inv_out.shape)
     inv_in[sp] = jnp.broadcast_to(inverse_row, inv_out.shape)
@@ -631,11 +678,23 @@
         def _():
             pass_copy(kind, origin, send_sem).start()
 
-    def arrive(kind, step):
-        await_piece(kind, sp, step)
-        if step == 2:
+    turn = lax.rem(chip + 1, 4) // 2
+    orders = (
+        chip,
+        hops[1] + turn * (hops[2] - hops[1]),
+        hops[2] + turn * (hops[1] - hops[2]),
+        hops[3],
+    )
+
+    def arrive(kind, number):
+        place = orders[number]
+        slot = rows[kind].at[sp, core, place]
+        remote(
+            slot, slot, mate_send.at[kind, sp], piece_recv.at[kind, sp, place], sp, mate
+        ).wait_recv()
+        if number == 1:
             pass_on(kind, sp, z_send.at[kind, 2])
-        send_piece(kind, step, rows[kind].at[sp, core, hops[step]])
+        send_piece(kind, number, slot, place)
 
     def corner_out(kind):
         await_piece(kind, corner, 0)
@@ -645,87 +704,388 @@
         def _():
             z_copy(kind, corner, 2, c_send.at[kind, 1]).start()
 
-    def corner_in(kind):
-        await_piece(kind, corner, 2)
-        pass_on(kind, corner, c_send.at[kind, 2])
-
+    def corner_over(kind):
+        @pl.when(middle)
+        def _():
+            await_piece(kind, corner, 2)
+            pass_copy(kind, corner, c_send.at[kind, 2]).start()
+
+    def await_pieces(kind, origin, steps):
+        for step in steps:
+            await_piece(kind, origin, step)
+
+    def await_corner(kind, steps):
+        await_pieces(kind, corner, steps)
+
+        @pl.when(edge)
+        def _():
+            await_piece(kind, corner, 2)
+
+    def mix():
+        sums = stat_out[...]
+        mean_row = sums[1:2] / channels
+        conv_std = to_column(lax.rsqrt(sums[2:3] / channels - mean_row * mean_row + EPSILON))
+        mean_val = to_column(mean_row)
+        ln_gain = ln_ref[...]
+        for begin in range(0, tokens, 64):
+            end = begin + 64
+            block = (conv_ref[begin:end].astype(jnp.float32) - mean_val[begin:end]) * conv_std[
+                begin:end
+            ]
+            scaled = block * ln_gain
+            logistic = 1.0 / (1.0 + jnp.exp(-scaled))
+            centred_ref[begin:end] = block
+            mixed_ref[begin:end] = (scaled * logistic).astype(jnp.bfloat16)
+            slope_ref[begin:end] = logistic * (1.0 + scaled * (1.0 - logistic)) * ln_gain
+        return conv_std
+
+    def turn_copy(group, i, h):
+        return remote(
+            turn_out.at[group, i, spans[h]],
+            turn_in.at[group, i, spans[h]],
+            turn_send.at[group, i, h],
+            turn_recv.at[group, i, h],
+            (along, across)[group],
+            tp,
+        )
+
+    def near_copy(side, i, h):
+        source, target = ((send_x, across), (send_y, along))[side]
+        return remote(
+            source.at[0, i, spans[h]],
+            near.at[side, i, spans[h]],
+            near_send.at[side, i, h],
+            near_recv.at[side, i, h],
+            target,
+            tp,
+        )
+
+    def far_copy(side, i, h):
+        source, target = ((send_x, across), (send_y, along))[side]
+        return remote(
+            source.at[1, i, spans[h]],
+            far.at[side, i, spans[h]],
+            far_send.at[side, i, h],
+            far_recv.at[side, i, h],
+            target,
+            tp,
+        )
+
+    def near_out(side, h):
+        for i in range(2):
+            go(near_copy(side, i, h))
+
+    def far_out(h):
+        for i in range(2):
+            for side in range(2):
+                go(far_copy(side, i, h))
+
+    def second_turn(h):
+        for i in range(2):
+            for group, off in ((0, 1 - row_of), (1, 1 - col_of)):
+                far_copy(group, i, h).wait_recv()
+                turn_out[group, i, spans[h]] = (
+                    keep[group, off, i, spans[h]].astype(jnp.float32)
+                    + far[group, i, spans[h]].astype(jnp.float32)
+                ).astype(jnp.bfloat16)
+                go(turn_copy(group, i, h))
+
+    def plane_sum(place, h):
+        group, i = place // 2, lax.rem(place, 2)
+        own = row_of + group * (col_of - row_of)
+        remote(
+            turn_in.at[group, i, spans[h]],
+            turn_in.at[group, i, spans[h]],
+            turn_send.at[group, i, h],
+            turn_recv.at[group, i, h],
+            sp,
+            mate,
+        ).wait_recv()
+        remote(
+            near.at[group, i, spans[h]],
+            near.at[group, i, spans[h]],
+            near_send.at[group, i, h],
+            near_recv.at[group, i, h],
+            sp,
+            mate,
+        ).wait_recv()
+        return (
+            keep[group, own, i, spans[h]].astype(jnp.float32)
+            + near[group, i, spans[h]].astype(jnp.float32)
+            + turn_in[group, i, spans[h]].astype(jnp.float32)
+        )
+
+    def r_copy(step, h):
+        return remote(
+            z_out.at[step, h],
+            z_in.at[chip, h],
+            r_send.at[step, h],
+            r_recv.at[chip, h],
+            sp,
+            2 * hops[step] + core,
+        )
+
+    def over_copy(h):
+        return remote(
+            z_out.at[2, h], over_in.at[h], r_send.at[2, h], over_recv.at[h], sp, 2 * hops[1] + core
+        )
+
+    def await_z(step, h):
+        slot = z_in.at[hops[step], h]
+        remote(slot, slot, r_send.at[0, h], r_recv.at[hops[step], h], sp, mate).wait_recv()
+
+    inner_rows = {}
+
+    def reduce_out(h):
+        inner = None
+        for step in (2, 3, 1, 0):
+            place = hops[step]
+            summed = plane_sum(place, h)
+            term = jnp.sum(
+                summed * rows_s[sp, core, place, spans[h]].astype(jnp.float32),
+                axis=1,
+                keepdims=True,
+            )
+            inner = term if inner is None else inner + term
+            if step == 0:
+                own_sum[spans[h]] = summed
+            elif step == 2:
+                over_sum[h] = summed
+                z_out[step, h] = summed.astype(jnp.bfloat16)
+            else:
+                z_out[step, h] = summed.astype(jnp.bfloat16)
+        row = to_row(inner)
+        inner_rows[h] = row
+        note_out[h] = jnp.broadcast_to(row, note_out.shape[1:])
+        for i, peer in enumerate(peers):
+            go(
+                remote(
+                    note_out.at[h], note_in.at[tp, h], note_send.at[i, h], note_recv.at[tp, h], sp, peer
+                )
+            )
+
+        @pl.when(edge)
+        def _():
+            over_copy(h).start()
+
+        for step in (3, 1):
+            go(r_copy(step, h))
+
+    def reduce_over(h):
+        @pl.when(middle)
+        def _():
+            slot = over_in.at[h]
+            remote(slot, slot, r_send.at[2, h], over_recv.at[h], sp, mate).wait_recv()
+            z_out[2, h] = (over_sum[h] + over_in[h].astype(jnp.float32)).astype(jnp.bfloat16)
+            r_copy(2, h).start()
+
+    def reduce_in(h):
+        for step in (1, 2):
+            await_z(step, h)
+        total = (
+            own_sum[spans[h]]
+            + z_in[hops[1], h].astype(jnp.float32)
+            + z_in[hops[2], h].astype(jnp.float32)
+        )
+        own_sum[spans[h]] = total
+
+        @pl.when(edge)
+        def _():
+            await_z(3, h)
+            own_sum[spans[h]] += z_in[hops[3], h].astype(jnp.float32)
+
+
+    def full_slot(place, h, half=None):
+        return full.at[core if half is None else half, place, spans[h]]
+
+    def full_copy(step, h):
+        slot = full_slot(chip, h)
+        return remote(
+            slot, slot, full_send.at[step - 1, h], full_recv.at[chip, h], sp, 2 * hops[step] + core
+        )
+
+    def full_pass(h):
+        slot = full_slot(hops[2], h)
+        return remote(
+            slot, slot, full_send.at[2, h], full_recv.at[hops[2], h], sp, 2 * hops[1] + core
+        )
+
+    def gather_out(h):
+        row = inner_rows[h]
+        for peer in peers:
+            slot = note_in.at[peer, h]
+            remote(slot, slot, note_send.at[0, h], note_recv.at[peer, h], sp, peer).wait_recv()
+            row = row + note_in[peer, h, 0:1]
+        scale = inv_col[h * half_rows : (h + 1) * half_rows]
+        factor = scale * scale * to_column(row) / width
+        full[core, chip, spans[h]] = (
+            up_ref[spans[h]].astype(jnp.float32)
+            + gain * own_sum[spans[h]]
+            - stream_ref[spans[h]].astype(jnp.float32) * factor
+        ).astype(jnp.bfloat16)
+
+        @pl.when(edge)
+        def _():
+            full_copy(3, h).start()
+
+        for step in (1, 2):
+            go(full_copy(step, h))
+
+    def mate_copy(place, h, half=None):
+        slot = full_slot(place, h, half)
+        return remote(slot, slot, fm_send.at[place, h], fm_recv.at[place, h], sp, mate)
+
+    def grad_copy(place, h):
+        return remote(
+            full_slot(place, h),
+            grads.at[sp, core, spans[h]],
+            grad_send.at[place, h],
+            grad_recv.at[sp, h],
+            place,
+            tp,
+        )
+
+    def mixed_term(half, place, h):
+        start = pl.multiple_of((2 * place + half) * columns, columns)
+        return dot_nt(full[half, place, spans[h]], w_out[:, pl.ds(start, columns)])
+
+    def fan(step, h):
+        place = hops[step]
+        if step > 0:
+            slot = full_slot(place, h)
+            remote(slot, slot, full_send.at[0, h], full_recv.at[place, h], sp, mate).wait_recv()
+        if step == 2:
+
+            @pl.when(middle)
+            def _():
+                full_pass(h).start()
+
+        mate_copy(place, h).start()
+
+        @pl.when(place != sp)
+        def _():
+            grad_copy(place, h).start()
+
+        term = mixed_term(core, place, h)
+        if step == 0:
+            mixed_back[spans[h]] = term
+        else:
+            mixed_back[spans[h]] += term
+
+    tails = []
+
+    def norm_out(h):
+        total = mixed_back[spans[h]]
+        for step in range(4):
+            place = hops[step]
+            mate_copy(place, h, 1 - core).wait_recv()
+            total = total + mixed_term(1 - core, place, h)
+        norm_in = total * slope_ref[spans[h]]
+        mixed_back[spans[h]] = norm_in
+        sums = jnp.concatenate(
+            [
+                to_row(jnp.sum(norm_in, axis=1, keepdims=True)),
+                to_row(jnp.sum(norm_in * centred_ref[spans[h]], axis=1, keepdims=True)),
+                jnp.zeros((6, half_rows), jnp.float32),
+            ],
+            axis=0,
+        )
+        tails.append(sums)
+        tail_out[h] = sums
+        for i, peer in enumerate(peers):
+            go(
+                remote(
+                    tail_out.at[h], tail_in.at[tp, h], tail_send.at[i, h], tail_recv.at[tp, h], sp, peer
+                )
+            )
+
+    def norm_back(h):
+        sums = tails[h]
+        for peer in peers:
+            slot = tail_in.at[peer, h]
+            remote(slot, slot, tail_send.at[0, h], tail_recv.at[peer, h], sp, peer).wait_recv()
+            sums = sums + tail_in[peer, h]
+        conv_out[spans[h]] = conv_std[h * half_rows : (h + 1) * half_rows] * (
+            mixed_back[spans[h]]
+            - to_column(sums[0:1]) / channels
+            - centred_ref[spans[h]] * (to_column(sums[1:2]) / channels)
+        )
+
+    def grads_in(h):
+        for other in others:
+            slot = grads.at[other, core, spans[h]]
+            remote(slot, slot, grad_send.at[0, h], grad_recv.at[other, h], other, tp).wait_recv()
+            go(
+                remote(
+                    slot, slot, gmate_send.at[other, h], gmate_recv.at[other, h], sp, mate
+                )
+            )
+
+    rim = rim_in.shape[0]
+    before = lax.rem(sp + 3, 4)
+    arrive(0, 1)
     relay(0, 0)
-    arrive(0, 1)
     relay(1, 0)
+    arrive(1, 1)
     arrive(0, 2)
     corner_out(0)
     arrive(0, 3)
+    arrive(1, 2)
+    corner_out(1)
     own_rows.wait()
     for load in loads:
         load.wait()
     share(0, sp)
     go(remote(wgu.at[:, 1 - core], mate_w, mw_sems.at[0], mw_sems.at[1], sp, mate))
-    corner_out(1)
-    arrive(1, 1)
     await_share(0, sp)
     forward(sp)
-    arrive(1, 2)
-    corner_in(0)
+    corner_over(0)
+    await_pieces(0, across, (1, 2, 3))
+    share(0, across)
+    await_share(0, across)
+    forward(across)
+    conv_std = mix()
+    own_mixed = pltpu.make_async_copy(mixed_ref, mixed.at[sp], local_sems.at[6])
+    relay(0, 3)
     arrive(1, 3)
     share(1, sp)
-    relay(0, 3)
-    for step in (1, 2, 3):
-        await_piece(0, across, step)
-    share(0, across)
-    for step in (0, 1, 2):
-        await_piece(0, along, step)
+    await_pieces(0, along, (0, 1, 2))
     share(0, along)
-    await_share(1, sp)
-    backward(sp)
-    corner_in(1)
-    await_share(0, across)
-    forward(across)
-    await_share(0, along)
-    forward(along)
     for other in others:
         for sems, landing in ((inv_recv, inv_in), (w_recv, w_in)):
             remote(
                 landing.at[other], landing.at[other], inv_send.at[0], sems.at[other], sp, mate
             ).wait_recv()
+    await_share(0, along)
+    forward(along)
+    await_share(1, sp)
+    backward(sp)
+    corner_over(1)
     activate(sp)
-    relay(1, 3)
-    for step in (1, 3):
-        await_piece(0, corner, step)
+    own_mixed.start()
+    inv_col = to_column(lax.rsqrt(stat_out[0:1] / width + EPSILON))
+    remote(mate_w, mate_w, mw_sems.at[0], mw_sems.at[1], sp, mate).wait_recv()
+    await_corner(0, (1, 3))
     share(0, corner)
     await_share(0, corner)
     forward(corner)
-    for step in (1, 2, 3):
-        await_piece(1, across, step)
+    relay(1, 3)
+    await_pieces(1, across, (1, 2, 3))
     share(1, across)
-    for step in (0, 1, 2):
-        await_piece(1, along, step)
-    share(1, along)
-    remote(mate_w, mate_w, mw_sems.at[0], mw_sems.at[1], sp, mate).wait_recv()
     await_share(1, across)
     backward(across)
     activate(across)
+    await_pieces(1, along, (0, 1, 2))
+    share(1, along)
+    spread(across, send_x.at[0], keep.at[1, 1 - col_of])
+    near_out(0, 0)
     await_share(1, along)
     backward(along)
     activate(along)
-    spread(across, send_x.at[0], keep.at[1, 1 - col_of])
-    for i in range(2):
-        go(
-            remote(
-                send_x.at[0, i], near_x_out.at[i], near_send.at[0, i], near_recv.at[0, i], across, tp
-            )
-        )
-    store(keep.at[1, 1 - col_of], keep_out.at[1, 1 - col_of], small_sems.at[2, 0])
+    spread(sp, keep.at[0, row_of], keep.at[1, col_of])
     spread(along, keep.at[0, 1 - row_of], send_y.at[0])
-    for i in range(2):
-        go(
-            remote(
-                send_y.at[0, i], near_y_out.at[i], near_send.at[1, i], near_recv.at[1, i], along, tp
-            )
-        )
-    store(keep.at[0, 1 - row_of], keep_out.at[0, 1 - row_of], small_sems.at[2, 1])
-    spread(sp, keep.at[0, row_of], keep.at[1, col_of])
-    store(keep.at[0, row_of], keep_out.at[0, row_of], small_sems.at[2, 2])
-    store(keep.at[1, col_of], keep_out.at[1, col_of], small_sems.at[2, 3])
+    near_out(1, 0)
+    await_corner(1, ())
     for step in (0, 1, 2, 3):
         place = hops[step]
         if step in (1, 3):
@@ -742,468 +1102,50 @@
     store(rows_u.at[corner, 1 - core], rows_u_out.at[corner, 1 - core], rows_sems.at[1, corner, 1])
     activate(corner)
     spread(corner, send_x.at[1], send_y.at[1])
-    store(send_x.at[1], far_x_out, small_sems.at[3, 0])
-    store(send_y.at[1], far_y_out, small_sems.at[3, 1])
-    for side, landing in enumerate((near_x_out, near_y_out)):
-        for i in range(2):
-            remote(
-                landing.at[i], landing.at[i], near_send.at[side, i], near_recv.at[side, i], sp, mate
-            ).wait_recv()
-    for copy in stores:
-        copy.wait()
-    for copy in pending:
-        copy.wait_send()
-    for kind in (0, 1):
-
-        @pl.when(edge)
-        def _(kind=kind):
-            z_copy(kind, sp, 3, z_send.at[kind, 2], owns[kind]).wait_send()
-
-        @pl.when(middle)
-        def _(kind=kind):
-            pass_copy(kind, sp, z_send.at[kind, 2]).wait_send()
-            z_copy(kind, corner, 2, c_send.at[kind, 1]).wait_send()
-            pass_copy(kind, corner, c_send.at[kind, 2]).wait_send()
-
-
-def grads_kernel(rows_s, rows_u, hidden, active, gate_out, up_out, down_out, tall, wide, sems):
-    columns = rows_s.shape[4]
-    part = active.shape[2]
-    pieces = 8
-
-    def copies(piece, slot):
-        span = pl.ds(pl.multiple_of(piece * columns, columns), columns)
-        return (
-            pltpu.make_async_copy(
-                tall.at[slot, :, pl.ds(0, part)], gate_out.at[span], sems.at[slot, 0]
-            ),
-            pltpu.make_async_copy(
-                tall.at[slot, :, pl.ds(part, part)], up_out.at[span], sems.at[slot, 1]
-            ),
-            pltpu.make_async_copy(wide.at[slot], down_out.at[:, span], sems.at[slot, 2]),
-        )
-
-    def body(piece, carry):
-        slot = lax.rem(piece, 2)
-        half, place = lax.rem(piece, 2), piece // 2
-
-        @pl.when(piece >= 2)
-        def _():
-            for copy in copies(piece - 2, slot):
-                copy.wait()
-
-        for origin in range(4):
-            tall_term = dot_tn(rows_s[origin, half, place], hidden[origin])
-            wide_term = dot_tn(active[origin], rows_u[origin, half, place])
-            if origin == 0:
-                tall[slot] = tall_term
-                wide[slot] = wide_term
-            else:
-                tall[slot] += tall_term
-                wide[slot] += wide_term
-        for copy in copies(piece, slot):
-            copy.start()
-        return carry
-
-    lax.fori_loop(0, pieces, body, 0)
-    for piece in (pieces - 2, pieces - 1):
-        for copy in copies(piece, piece % 2):
-            copy.wait()
-
-
-def return_kernel(
-    width,
-    channels,
-    keep_hbm,
-    far_x_hbm,
-    far_y_hbm,
-    near_x_hbm,
-    near_y_hbm,
-    up_ref,
-    stream_ref,
-    gain_ref,
-    stat_ref,
-    conv_ref,
-    ln_ref,
-    w_hbm,
-    conv_out,
-    grads,
-    mixed,
-    w_out,
-    keep,
-    far,
-    near,
-    mixed_ref,
-    slope_ref,
-    centred_ref,
-    turn_out,
-    turn_in,
-    z_out,
-    z_in,
-    over_in,
-    over_sum,
-    own_sum,
-    mixed_back,
-    note_out,
-    note_in,
-    tail_out,
-    tail_in,
-    full,
-    rim_in,
-    mix_send,
-    mix_recv,
-    turn_send,
-    turn_recv,
-    z_send,
-    z_recv,
-    over_recv,
-    note_send,
-    note_recv,
-    tail_send,
-    tail_recv,
-    full_send,
-    full_recv,
-    mate_send,
-    mate_recv,
-    grad_send,
-    grad_recv,
-    gmate_send,
-    gmate_recv,
-    rim_sems,
-    local_sems,
-):
-    sp, tp, chip, core, across, along, corner, hops = places()
-    mate = tp + 1 - 2 * core
-    tp_count = 8
-    tokens, columns = up_ref.shape
-    row_of = sp // 2
-    col_of = lax.rem(sp, 2)
-    peers = [lax.rem(tp + step, tp_count) for step in range(1, tp_count)]
-    others = (across, along, corner)
-    signal([(sp, peer) for peer in peers] + [(other, tp) for other in others])
-    pulls = [
-        pltpu.make_async_copy(source, target, local_sems.at[2 + i])
-        for i, (source, target) in enumerate(
-            (
-                (far_x_hbm, far.at[0]),
-                (far_y_hbm, far.at[1]),
-                (keep_hbm, keep),
-                (near_x_hbm, near.at[0]),
-                (near_y_hbm, near.at[1]),
-            )
-        )
-    ]
-    for pull in pulls:
-        pull.start()
-    load = pltpu.make_async_copy(w_hbm, w_out, local_sems.at[0])
-    load.start()
-    inverse = to_column(lax.rsqrt(stat_ref[0:1] / width + EPSILON))
-    mean_row = stat_ref[1:2] / channels
-    inv_std = to_column(lax.rsqrt(stat_ref[2:3] / channels - mean_row * mean_row + EPSILON))
-    mean_val = to_column(mean_row)
-    ln_gain = ln_ref[...]
-    for begin in range(0, tokens, 64):
-        end = begin + 64
-        block = (conv_ref[begin:end].astype(jnp.float32) - mean_val[begin:end]) * inv_std[
-            begin:end
-        ]
-        scaled = block * ln_gain
-        logistic = 1.0 / (1.0 + jnp.exp(-scaled))
-        centred_ref[begin:end] = block
-        mixed_ref[begin:end] = (scaled * logistic).astype(jnp.bfloat16)
-        slope_ref[begin:end] = logistic * (1.0 + scaled * (1.0 - logistic)) * ln_gain
-    await_signals(len(peers) + len(others))
-    own_mixed = pltpu.make_async_copy(mixed_ref, mixed.at[sp], local_sems.at[1])
-    own_mixed.start()
-    for pull in pulls:
-        pull.wait()
-    pending = []
-
-    def go(copy):
-        copy.start()
-        pending.append(copy)
-
-    edge = lax.rem(chip + 1, 4) // 2 == 0
-    middle = jnp.logical_not(edge)
-    halves = 2
-    half_rows = tokens // halves
-    spans = [pl.ds(h * half_rows, half_rows) for h in range(halves)]
-
-    def turn_copy(group, i, h):
-        return remote(
-            turn_out.at[group, i, spans[h]],
-            turn_in.at[group, i, spans[h]],
-            turn_send.at[group, i, h],
-            turn_recv.at[group, i, h],
-            (along, across)[group] if isinstance(group, int) else sp,
-            tp,
-        )
-
-    for h in range(halves):
-        for i in range(2):
-            for group, off in ((0, 1 - row_of), (1, 1 - col_of)):
-                turn_out[group, i, spans[h]] = (
-                    keep[group, off, i, spans[h]].astype(jnp.float32)
-                    + far[group, i, spans[h]].astype(jnp.float32)
-                ).astype(jnp.bfloat16)
-                go(turn_copy(group, i, h))
+    rim = rim_in.shape[0]
+    before = lax.rem(sp + 3, 4)
+    far_out(0)
+    second_turn(0)
+    for side in range(2):
+        near_out(side, 1)
+    far_out(1)
+    reduce_out(0)
+    second_turn(1)
+    reduce_over(0)
+    reduce_in(0)
+    gather_out(0)
+    out_load.wait()
+    fan(0, 0)
+    reduce_out(1)
+    fan(2, 0)
+    reduce_over(1)
+    fan(1, 0)
+    reduce_in(1)
+    fan(3, 0)
+    gather_out(1)
+    own_mixed.wait()
     for i, other in enumerate(others):
         go(remote(mixed_ref, mixed.at[sp], mix_send.at[i], mix_recv.at[sp], other, tp))
-
-    def plane_sum(place, h):
-        group, i = place // 2, lax.rem(place, 2)
-        own = row_of + group * (col_of - row_of)
-        remote(
-            turn_in.at[group, i, spans[h]],
-            turn_in.at[group, i, spans[h]],
-            turn_send.at[group, i, h],
-            turn_recv.at[group, i, h],
-            sp,
-            mate,
-        ).wait_recv()
-        return (
-            keep[group, own, i, spans[h]].astype(jnp.float32)
-            + near[group, i, spans[h]].astype(jnp.float32)
-            + turn_in[group, i, spans[h]].astype(jnp.float32)
-        )
-
-    def z_copy(step, h):
-        return remote(
-            z_out.at[step, h],
-            z_in.at[chip, h],
-            z_send.at[step, h],
-            z_recv.at[chip, h],
-            sp,
-            2 * hops[step] + core,
-        )
-
-    def over_copy(h):
-        return remote(
-            z_out.at[2, h], over_in.at[h], z_send.at[2, h], over_recv.at[h], sp, 2 * hops[1] + core
-        )
-
-    def await_z(step, h):
-        slot = z_in.at[hops[step], h]
-        remote(slot, slot, z_send.at[0, h], z_recv.at[hops[step], h], sp, mate).wait_recv()
-
-    def reduce_out(h):
-        summed = plane_sum(hops[2], h)
-
-        @pl.when(edge)
-        def _():
-            z_out[2, h] = summed.astype(jnp.bfloat16)
-            over_copy(h).start()
-
-        @pl.when(middle)
-        def _():
-            over_sum[h] = summed
-
-        for step in (3, 1):
-            z_out[step, h] = plane_sum(hops[step], h).astype(jnp.bfloat16)
-            go(z_copy(step, h))
-        own_sum[spans[h]] = plane_sum(chip, h)
-
-    def reduce_over(h):
-        @pl.when(middle)
-        def _():
-            slot = over_in.at[h]
-            remote(slot, slot, z_send.at[2, h], over_recv.at[h], sp, mate).wait_recv()
-            z_out[2, h] = (over_sum[h] + over_in[h].astype(jnp.float32)).astype(jnp.bfloat16)
-            z_copy(2, h).start()
-
-    gain = gain_ref[...]
-    inner_rows = []
-
-    def reduce_in(h):
-        for step in (1, 2):
-            await_z(step, h)
-        total = (
-            own_sum[spans[h]]
-            + z_in[hops[1], h].astype(jnp.float32)
-            + z_in[hops[2], h].astype(jnp.float32)
-        )
-        own_sum[spans[h]] = total
-
-        @pl.when(edge)
-        def _():
-            await_z(3, h)
-            own_sum[spans[h]] += z_in[hops[3], h].astype(jnp.float32)
-
-        gained = gain * own_sum[spans[h]]
-        own_sum[spans[h]] = gained
-        row = to_row(
-            jnp.sum(gained * stream_ref[spans[h]].astype(jnp.float32), axis=1, keepdims=True)
-        )
-        inner_rows.append(row)
-        note_out[h] = jnp.broadcast_to(row, note_out.shape[1:])
-        for i, peer in enumerate(peers):
-            go(
-                remote(
-                    note_out.at[h], note_in.at[tp, h], note_send.at[i, h], note_recv.at[tp, h], sp, peer
-                )
-            )
-
-    def full_slot(place, h, half=None):
-        return full.at[core if half is None else half, place, spans[h]]
-
-    def full_copy(step, h):
-        slot = full_slot(chip, h)
-        return remote(
-            slot, slot, full_send.at[step - 1, h], full_recv.at[chip, h], sp, 2 * hops[step] + core
-        )
-
-    def full_pass(h):
-        slot = full_slot(hops[2], h)
-        return remote(
-            slot, slot, full_send.at[2, h], full_recv.at[hops[2], h], sp, 2 * hops[1] + core
-        )
-
-    def gather_out(h):
-        row = inner_rows[h]
-        for peer in peers:
-            slot = note_in.at[peer, h]
-            remote(slot, slot, note_send.at[0, h], note_recv.at[peer, h], sp, peer).wait_recv()
-            row = row + note_in[peer, h, 0:1]
-        scale = inverse[h * half_rows : (h + 1) * half_rows]
-        factor = scale * scale * to_column(row) / width
-        full[core, chip, spans[h]] = (
-            up_ref[spans[h]].astype(jnp.float32)
-            + own_sum[spans[h]]
-            - stream_ref[spans[h]].astype(jnp.float32) * factor
-        ).astype(jnp.bfloat16)
-        for step in (1, 2):
-            go(full_copy(step, h))
-
-        @pl.when(edge)
-        def _():
-            full_copy(3, h).start()
-
-    def mate_copy(place, h, half=None):
-        slot = full_slot(place, h, half)
-        return remote(slot, slot, mate_send.at[place, h], mate_recv.at[place, h], sp, mate)
-
-    def grad_copy(place, h):
-        return remote(
-            full_slot(place, h),
-            grads.at[sp, core, spans[h]],
-            grad_send.at[place, h],
-            grad_recv.at[sp, h],
-            place,
-            tp,
-        )
-
-    def mixed_term(half, place, h):
-        start = pl.multiple_of((2 * place + half) * columns, columns)
-        return dot_nt(full[half, place, spans[h]], w_out[:, pl.ds(start, columns)])
-
-    def fan(step, h):
-        place = hops[step]
-        if step > 0:
-            slot = full_slot(place, h)
-            remote(slot, slot, full_send.at[0, h], full_recv.at[place, h], sp, mate).wait_recv()
-        if step == 2:
-
-            @pl.when(middle)
-            def _():
-                full_pass(h).start()
-
-        mate_copy(place, h).start()
-
-        @pl.when(place != sp)
-        def _():
-            grad_copy(place, h).start()
-
-        term = mixed_term(core, place, h)
-        if step == 0:
-            mixed_back[spans[h]] = term
-        else:
-            mixed_back[spans[h]] += term
-
-    tails = []
-
-    def norm_out(h):
-        total = mixed_back[spans[h]]
-        for step in range(4):
-            place = hops[step]
-            mate_copy(place, h, 1 - core).wait_recv()
-            total = total + mixed_term(1 - core, place, h)
-        norm_in = total * slope_ref[spans[h]]
-        mixed_back[spans[h]] = norm_in
-        sums = jnp.concatenate(
-            [
-                to_row(jnp.sum(norm_in, axis=1, keepdims=True)),
-                to_row(jnp.sum(norm_in * centred_ref[spans[h]], axis=1, keepdims=True)),
-                jnp.zeros((6, half_rows), jnp.float32),
-            ],
-            axis=0,
-        )
-        tails.append(sums)
-        tail_out[h] = sums
-        for i, peer in enumerate(peers):
-            go(
-                remote(
-                    tail_out.at[h], tail_in.at[tp, h], tail_send.at[i, h], tail_recv.at[tp, h], sp, peer
-                )
-            )
-
-    def norm_back(h):
-        sums = tails[h]
-        for peer in peers:
-            slot = tail_in.at[peer, h]
-            remote(slot, slot, tail_send.at[0, h], tail_recv.at[peer, h], sp, peer).wait_recv()
-            sums = sums + tail_in[peer, h]
-        conv_out[spans[h]] = inv_std[h * half_rows : (h + 1) * half_rows] * (
-            mixed_back[spans[h]]
-            - to_column(sums[0:1]) / channels
-            - centred_ref[spans[h]] * (to_column(sums[1:2]) / channels)
-        )
-
-    def grads_in(h):
-        for other in others:
-            slot = grads.at[other, core, spans[h]]
-            remote(slot, slot, grad_send.at[0, h], grad_recv.at[other, h], other, tp).wait_recv()
-            go(
-                remote(
-                    slot, slot, gmate_send.at[other, h], gmate_recv.at[other, h], sp, mate
-                )
-            )
-
-    rim = rim_in.shape[0]
-    before = lax.rem(sp + 3, 4)
-    reduce_out(0)
-    reduce_out(1)
-    reduce_over(0)
-    reduce_over(1)
-    reduce_in(0)
-    gather_out(0)
-    reduce_in(1)
-    load.wait()
-    fan(0, 0)
-    fan(1, 0)
-    gather_out(1)
-    fan(2, 0)
-    fan(3, 0)
+    norm_out(0)
+    grads_in(0)
     fan(0, 1)
+    fan(2, 1)
     fan(1, 1)
-    norm_out(0)
-    fan(2, 1)
+    fan(3, 1)
     norm_back(0)
     go(
         remote(
             conv_out.at[pl.ds(0, rim)], rim_in, rim_sems.at[0], rim_sems.at[1], before, tp
         )
     )
-    grads_in(0)
-    own_mixed.wait()
+    norm_out(1)
+    grads_in(1)
+    for half in range(2):
+        grads[sp, half] = full[half, sp]
+    norm_back(1)
     for other in others:
         slot = mixed.at[other]
         remote(slot, slot, mix_send.at[0], mix_recv.at[other], other, tp).wait_recv()
-    fan(3, 1)
-    norm_out(1)
-    for half in range(2):
-        grads[sp, half] = full[half, sp]
-    grads_in(1)
-    norm_back(1)
     remote(rim_in, rim_in, rim_sems.at[0], rim_sems.at[1], before, tp).wait_recv()
     last = (sp < 3).astype(jnp.float32)
     conv_out[tokens : tokens + rim] = rim_in[...] * last
@@ -1228,36 +1170,78 @@
 
         @pl.when(middle)
         def _(h=h):
-            z_copy(2, h).wait_send()
+            r_copy(2, h).wait_send()
             full_pass(h).wait_send()
 
+    for copy in stores:
+        copy.wait()
     for copy in pending:
         copy.wait_send()
-
-
-def finish_kernel(conv, taps, value_in, gate_in, grads, mixed, grad_out, value_out, gate_out):
+    for kind in (0, 1):
+
+        @pl.when(edge)
+        def _(kind=kind):
+            z_copy(kind, sp, 3, z_send.at[kind, 2], owns[kind]).wait_send()
+
+        @pl.when(middle)
+        def _(kind=kind):
+            pass_copy(kind, sp, z_send.at[kind, 2]).wait_send()
+            z_copy(kind, corner, 2, c_send.at[kind, 1]).wait_send()
+            pass_copy(kind, corner, c_send.at[kind, 2]).wait_send()
+
+
+def finish_kernel(
+    rows_s,
+    rows_u,
+    hidden,
+    active,
+    conv,
+    taps,
+    value_in,
+    gate_in,
+    grads,
+    mixed,
+    grad_gate,
+    grad_up,
+    grad_down,
+    grad_out,
+    value_out,
+    gate_out,
+):
+    step = pl.program_id(0)
     tokens, part = value_in.shape
     tap_count = taps.shape[0]
-    columns = grads.shape[3]
-    for half in range(2):
-        total = dot_tn(mixed[0], grads[0, half])
-        for origin in range(1, 4):
-            total = total + dot_tn(mixed[origin], grads[origin, half])
-        grad_out[:, half * columns : (half + 1) * columns] = total
-    glu = jnp.zeros((tokens, part), jnp.float32)
-    for residue in range(8):
-        rolled = None
-        for offset in range(residue, tap_count, 8):
-            base = offset - residue
-            tap = taps[tap_count - 1 - offset : tap_count - offset]
-            term = tap * conv[base : base + tokens + 8]
-            rolled = term if rolled is None else rolled + term
-        glu = glu + rolled[residue : residue + tokens]
-    sigma = 1.0 / (1.0 + jnp.exp(-gate_in[...].astype(jnp.float32)))
-    value_out[...] = (glu * sigma).astype(jnp.bfloat16)
-    gate_out[...] = (
-        glu * value_in[...].astype(jnp.float32) * sigma * (1.0 - sigma)
-    ).astype(jnp.bfloat16)
+    tall = all_rows(hidden[...])
+    term = dot_tn(all_rows(rows_s[:, 0, 0]), tall)
+    half = term.shape[1] // 2
+    grad_gate[...] = term[:, :half]
+    grad_up[...] = term[:, half:]
+    grad_down[...] = dot_tn(all_rows(active[...]), all_rows(rows_u[:, 0, 0]))
+
+    @pl.when(lax.rem(step, 4) == 3)
+    def _():
+        grad_out[...] = dot_tn(all_rows(mixed[...]), all_rows(grads[:, 0]))
+
+    @pl.when(step == 1)
+    def _():
+        glu = jnp.zeros((tokens, part), jnp.float32)
+        for residue in range(8):
+            rolled = None
+            for offset in range(residue, tap_count, 8):
+                base = offset - residue
+                tap = taps[tap_count - 1 - offset : tap_count - offset]
+                product = tap * conv[base : base + tokens + 8]
+                rolled = product if rolled is None else rolled + product
+            glu = glu + rolled[residue : residue + tokens]
+        sigma = 1.0 / (1.0 + jnp.exp(-gate_in[...].astype(jnp.float32)))
+        value_out[...] = (glu * sigma).astype(jnp.bfloat16)
+        gate_out[...] = (
+            glu * value_in[...].astype(jnp.float32) * sigma * (1.0 - sigma)
+        ).astype(jnp.bfloat16)
+
+
+def all_rows(blocks):
+    return blocks.reshape(blocks.shape[0] * blocks.shape[1], blocks.shape[2])
 
 
 def fused_device(
@@ -1292,22 +1276,20 @@
 
     piece = (chips, 2, columns, part)
     rows_shape = (sp_count, 2, chips, tokens, columns)
-    outs = pl.pallas_call(
-        functools.partial(expert_kernel, width),
+    rim = -(-(conv_taps.shape[0] - 1) // 8) * 8
+    rows_s, rows_u, hidden, active, conv_back, grads, mixed = pl.pallas_call(
+        functools.partial(step_kernel, width, channels),
         out_shape=(
             shape(rows_shape, bf16),
             shape(rows_shape, bf16),
             shape((sp_count, tokens, 2 * part), bf16),
             shape((sp_count, tokens, part), bf16),
-            shape((2, 2, 2, tokens, columns), bf16),
-            shape((2, tokens, columns), bf16),
-            shape((2, tokens, columns), bf16),
-            shape((2, tokens, columns), bf16),
-            shape((2, tokens, columns), bf16),
-            shape((8, tokens), f32),
+            shape((tokens + rim, channel_part), f32),
+            shape((sp_count, 2, tokens, columns), bf16),
+            shape((sp_count, tokens, channel_part), bf16),
         ),
-        in_specs=[vmem] * 6 + [anywhere] * 3,
-        out_specs=[anywhere] * 9 + [vmem],
+        in_specs=[vmem] * 7 + [anywhere] * 4,
+        out_specs=[anywhere] * 4 + [vmem] * 3,
         scratch_shapes=[
             pltpu.VMEM(rows_shape, bf16),
             pltpu.VMEM(rows_shape, bf16),
@@ -1316,7 +1298,10 @@
             pltpu.VMEM((2, 2, 2, tokens, columns), bf16),
             pltpu.VMEM((2, 2, tokens, columns), bf16),
             pltpu.VMEM((2, 2, tokens, columns), bf16),
+            pltpu.VMEM((2, 2, tokens, columns), bf16),
+            pltpu.VMEM((2, 2, tokens, columns), bf16),
             pltpu.VMEM((tokens, columns), bf16),
+            pltpu.VMEM((8, tokens), f32),
             pltpu.VMEM((8, tokens), f32),
             pltpu.VMEM((sp_count, 8, tokens), f32),
             pltpu.VMEM((chips, 2, columns, 2 * part), bf16),
@@ -1329,91 +1314,7 @@
             pltpu.VMEM((8, tokens), f32),
             pltpu.VMEM((sp_count, 8, tokens), f32),
             pltpu.VMEM((sp_count, 8, tokens), f32),
-            dma((2, 3)),
-            dma((2, sp_count, chips)),
-            dma((2, chips, 2)),
-            dma((2, chips)),
-            dma((2, sp_count)),
-            dma((2, sp_count)),
-            dma((chips,)),
-            dma((chips,)),
-            dma((2, 3)),
-            dma((2, 2)),
-            dma((2, 2)),
-            dma((tp_count - 1,)),
-            dma((tp_count,)),
-            dma((3,)),
-            dma((sp_count,)),
-            dma((3,)),
-            dma((sp_count,)),
-            dma((2,)),
-            dma((sp_count,)),
-            dma((sp_count,)),
-            dma((5,)),
-            dma((2, sp_count, 2)),
-            dma((4, sp_count)),
-        ],
-        compiler_params=pltpu.CompilerParams(
-            collective_id=3, has_side_effects=True, vmem_limit_bytes=VMEM_LIMIT
-        ),
-        cost_estimate=pl.CostEstimate(
-            flops=10**10, bytes_accessed=10**8, transcendentals=0
-        ),
-        name="expert_gather",
-    )(
-        stream,
-        upstream,
-        norm_gain[None, :],
-        routes.T,
-        route_weights.T,
-        conv_pre,
-        w_gate[0].reshape(piece),
-        w_up[0].reshape(piece),
-        w_down[0],
-    )
-    rows_s, rows_u, hidden, active, keep, far_x, far_y, near_x, near_y, totals = outs
-
-    def swap(block, step):
-        route = [(i, i + step if (i // step) % 2 == 0 else i - step) for i in range(sp_count)]
-        return lax.ppermute(block, "sp", route)
-
-    got_x = swap(far_x, 1)
-    got_y = swap(far_y, 2)
-
-    grad_gate, grad_up, grad_down = pl.pallas_call(
-        grads_kernel,
-        out_shape=(shape((width, part), f32), shape((width, part), f32), shape((part, width), f32)),
-        in_specs=[vmem] * 4,
-        out_specs=[anywhere] * 3,
-        scratch_shapes=[
-            pltpu.VMEM((2, columns, 2 * part), f32),
-            pltpu.VMEM((2, part, columns), f32),
-            dma((2, 3)),
-        ],
-        compiler_params=pltpu.CompilerParams(vmem_limit_bytes=VMEM_LIMIT),
-        cost_estimate=pl.CostEstimate(
-            flops=6 * width * part * tokens * sp_count,
-            bytes_accessed=40 * 2**20,
-            transcendentals=0,
-        ),
-        name="weight_grads",
-    )(rows_s, rows_u, hidden, active)
-
-    rim = -(-(conv_taps.shape[0] - 1) // 8) * 8
-    conv_back, grads, mixed = pl.pallas_call(
-        functools.partial(return_kernel, width, channels),
-        out_shape=(
-            shape((tokens + rim, channel_part), f32),
-            shape((sp_count, 2, tokens, columns), bf16),
-            shape((sp_count, tokens, channel_part), bf16),
-        ),
-        in_specs=[anywhere] * 5 + [vmem] * 6 + [anywhere],
-        out_specs=[vmem] * 3,
-        scratch_shapes=[
             pltpu.VMEM(w_out.shape, bf16),
-            pltpu.VMEM((2, 2, 2, tokens, columns), bf16),
-            pltpu.VMEM((2, 2, tokens, columns), bf16),
-            pltpu.VMEM((2, 2, tokens, columns), bf16),
             pltpu.VMEM((tokens, channel_part), bf16),
             pltpu.VMEM((tokens, channel_part), f32),
             pltpu.VMEM((tokens, channel_part), f32),
@@ -1431,6 +1332,31 @@
             pltpu.VMEM((tp_count, 2, 8, tokens // 2), f32),
             pltpu.VMEM((2, chips, tokens, columns), bf16),
             pltpu.VMEM((rim, channel_part), f32),
+            dma((2, 3)),
+            dma((2, sp_count, chips)),
+            dma((2, chips, 2)),
+            dma((2, chips)),
+            dma((2, sp_count)),
+            dma((2, sp_count)),
+            dma((chips,)),
+            dma((chips,)),
+            dma((2, 3)),
+            dma((2, 2, 2)),
+            dma((2, 2, 2)),
+            dma((2, 2, 2)),
+            dma((2, 2, 2)),
+            dma((tp_count - 1,)),
+            dma((tp_count,)),
+            dma((3,)),
+            dma((sp_count,)),
+            dma((3,)),
+            dma((sp_count,)),
+            dma((2,)),
+            dma((sp_count,)),
+            dma((sp_count,)),
+            dma((7,)),
+            dma((2, sp_count, 2)),
+            dma((2, sp_count)),
             dma((3,)),
             dma((sp_count,)),
             dma((2, 2, 2)),
@@ -1451,44 +1377,86 @@
             dma((sp_count, 2)),
             dma((sp_count, 2)),
             dma((2,)),
-            dma((7,)),
         ],
         compiler_params=pltpu.CompilerParams(
-            collective_id=4, has_side_effects=True, vmem_limit_bytes=VMEM_LIMIT
+            collective_id=3, has_side_effects=True, vmem_limit_bytes=VMEM_LIMIT
         ),
         cost_estimate=pl.CostEstimate(
             flops=10**10, bytes_accessed=10**8, transcendentals=0
         ),
-        name="return_path",
+        name="routed_step",
     )(
-        keep,
-        got_x,
-        got_y,
-        near_x,
-        near_y,
+        stream,
         upstream,
-        stream,
         norm_gain[None, :],
-        totals,
+        routes.T,
+        route_weights.T,
         conv_pre,
         ln_gain[None, :],
+        w_gate[0].reshape(piece),
+        w_up[0].reshape(piece),
+        w_down[0],
         w_out,
     )
-    grad_out, value_grad, gate_grad = pl.pallas_call(
+
+    def fixed(count):
+        return lambda step: (0,) * count
+
+    piece_spec = pl.BlockSpec(
+        (sp_count, 1, 1, tokens, columns), lambda step: (0, step % 2, step // 2, 0, 0)
+    )
+    grad_gate, grad_up, grad_down, grad_out, value_grad, gate_grad = pl.pallas_call(
         finish_kernel,
+        grid=(tp_count,),
         out_shape=(
+            shape((width, part), f32),
+            shape((width, part), f32),
+            shape((part, width), f32),
             shape((channel_part, 2 * columns), f32),
             shape((tokens, channel_part), bf16),
             shape((tokens, channel_part), bf16),
         ),
-        in_specs=[vmem] * 6,
-        out_specs=[vmem] * 3,
+        in_specs=[
+            piece_spec,
+            piece_spec,
+            pl.BlockSpec(hidden.shape, fixed(3)),
+            pl.BlockSpec(active.shape, fixed(3)),
+            pl.BlockSpec(conv_back.shape, fixed(2)),
+            pl.BlockSpec(conv_taps.shape, fixed(2)),
+            pl.BlockSpec(value_in.shape, fixed(2)),
+            pl.BlockSpec(gate_in.shape, fixed(2)),
+            pl.BlockSpec(
+                (sp_count, 1, tokens, columns), lambda step: (0, step // 4, 0, 0)
+            ),
+            pl.BlockSpec(mixed.shape, fixed(3)),
+        ],
+        out_specs=[
+            pl.BlockSpec((columns, part), lambda step: (step, 0)),
+            pl.BlockSpec((columns, part), lambda step: (step, 0)),
+            pl.BlockSpec((part, columns), lambda step: (0, step)),
+            pl.BlockSpec((channel_part, columns), lambda step: (0, step // 4)),
+            pl.BlockSpec((tokens, channel_part), fixed(2)),
+            pl.BlockSpec((tokens, channel_part), fixed(2)),
+        ],
         compiler_params=pltpu.CompilerParams(vmem_limit_bytes=VMEM_LIMIT),
         cost_estimate=pl.CostEstimate(
-            flops=10**9, bytes_accessed=10**7, transcendentals=0
+            flops=6 * width * part * tokens * sp_count,
+            bytes_accessed=40 * 2**20,
+            transcendentals=0,
         ),
         name="finish",
-    )(conv_back, conv_taps, value_in, gate_in, grads, mixed)
+    )(
+        rows_s,
+        rows_u,
+        hidden,
+        active,
+        conv_back,
+        conv_taps,
+        value_in,
+        gate_in,
+        grads,
+        mixed,
+    )
     return (grad_gate[None], grad_up[None], grad_down[None], grad_out, value_grad, gate_grad)
 
 

time: 195 us -> 185 us (0.949)
  Pallas kernels: 191 us -> 183 us
    pallas_call x4 -> x2, Pallas kernels: 191 us -> 183 us  [the longest x1 164 us: fused_device(): pl.pallas_call(functools.partial(step_kernel, width, channels), out_shape...]
  transfers between devices with their start and end apart: 2 -> 0, of which waited for: 0 -> 0; matrix products, arithmetic and copies ran while one was open for 0% -> 0% of each run, Pallas kernels for 8% -> 0%
where the time goes in v2:
time: 185 us; the launch traced here: 184 us
  Pallas kernels  183 us (99%)
    pallas_call x1, Pallas kernels, fused_device(): pl.pallas_call(functools.partial(step_kernel, width, channels), out_shape...  164 us
    pallas_call x1, Pallas kernels, fused_device(): pl.pallas_call(finish_kernel, grid=(tp_count,), out_shape=(shape((width,...  18.4 us

profile of v2, /device:TPU:0, one launch (start us, length us, event | category | flops | bytes accessed | tf_op | source)
XLA Modules:
  0.0 183.6 jit_solution(7817792838394702521)
XLA Ops:
  0.6 164.4 %routed_step.1 = (bf16[4,2,4,256,512]{4,3,2,1,0:T(8,128)(2,1)}, bf16[4,2,4,256,512]{4,3,2,1,0:T(8,128)(2,1)}, bf16[4,256,512]{2,1,0:T(8,128)(2,1)}, bf16[4,256,2...) custom-call(bf16[256,512]{1,0:T(8,128)(2,1)} %stream_ref.1, ...), custom_call_target="tpu_custom_call" | custom-call | flops 10000000000 | bytes 100000000 | tf_op jit(solution)/shard_map/routed_step/pallas_call | solution.py:1280
  165.0 18.4 %finish.1 = (f32[4096,256]{1,0:T(8,128)}, f32[4096,256]{1,0:T(8,128)}, f32[256,4096]{1,0:T(8,128)}, f32[256,1024]{1,0:T(8,128)}, bf16[256,256]{1,0:T(8,128)(2,1)}, /*index=5*/bf16[256,256]{1,0:T(8,128)(2,1)}) custom-call(bf16[4,2,4,256,512]{4,3,2,1,0:T(8,128)(2,1)} %get-tuple-element.19.rows_s, bf16[4,2,4,256,512]{4,3,2,1,0:T(8,128)(2,1)} %get-tuple-element.20.rows_u, ...), custom_call_target="tpu_custom_call" | custom-call | flops 6442450944 | bytes 41943040 | tf_op jit(solution)/shard_map/finish/pallas_call | solution.py:1408
